TPU v7x, 32 devices: a whole 2x2x4 slice. The times are simulated.
32 devices in a mesh: sp: 4 (over y, x), tp: 8 (over z, core).
Axes of the slice: x: 2, y: 2, z: 4, core: 2. Of those that a mesh axis runs over, the one named last changes fastest.
Arguments:
- layer_input: bfloat16 [1024, 4096], P('sp', 'tp'), may hold values from -6 to 6
- out_cotangent: bfloat16 [1024, 4096], P('sp', 'tp'), may hold values from -1.5 to 1.5
- routes: int32 [1024, 2], P('sp'), may hold values from 0 to 3, all different within a row; in each aligned block of 256 rows (0 to 255, 256 to 511, ...) at most 160 rows name the same one
- route_weights: float32 [1024, 2], P('sp'), may hold values from 0.2 to 1
- gate_proj: bfloat16 [4, 4096, 2048], P('sp', None, 'tp'), may hold values from -0.09375 to 0.09375
- up_proj: bfloat16 [4, 4096, 2048], P('sp', None, 'tp'), may hold values from -0.09375 to 0.09375
- down_proj: bfloat16 [4, 2048, 4096], P('sp', 'tp'), may hold values from -0.125 to 0.125
- out_proj: bfloat16 [4096, 4096], P(None, 'tp'), may hold values from -0.09375 to 0.09375
- mixer_output: bfloat16 [1024, 4096], P('sp', 'tp'), may hold values from -0.29882812 to 0.29882812
- queries: bfloat16 [1024, 2048], P('sp', 'tp'), may hold values from -6 to 6
- key_rows: bfloat16 [1024, 2048], P('sp', 'tp'), may hold values from -6 to 6
- value_rows: bfloat16 [1024, 4096], P('sp', 'tp'), may hold values from -0.3984375 to 0.3984375
- log_decay: float32 [1024, 2048], P('sp', 'tp'), may hold values from -1.5 to 0, as said below
- entry_state: float32 [4, 16, 128, 256], P('sp', 'tp'), may hold values from -6 to 6
Outputs:
- gate_proj_grad: bfloat16 [4, 4096, 2048], P('sp', None, 'tp')
- up_proj_grad: bfloat16 [4, 4096, 2048], P('sp', None, 'tp')
- down_proj_grad: bfloat16 [4, 2048, 4096], P('sp', 'tp')
- out_proj_grad: float32 [4096, 4096], P('sp', 'tp')
- query_grad: bfloat16 [1024, 2048], P('sp', 'tp')
- key_grad: bfloat16 [1024, 2048], P('sp', 'tp')
- value_grad: bfloat16 [1024, 4096], P('sp', 'tp')
- decay_grad: float32 [1024, 2048], P('sp', 'tp')
Inputs may be any that keep to these rules, and one draw needn't show every extreme that they name: `routes`: each token names 2 different experts. Among the tokens of one index of sp no expert is named more than 160 times, and in every draw some expert is named exactly 160 times by the tokens of some index of sp. `log_decay`: every entry is negative.
All inputs are finite; a program needn't handle non-finite values.
Results may differ from a plain program's by a relative error of at most 0.022.
Values may be sent and summed in bfloat16 or wider, within the bound.
A program may use at most 128 MiB of HBM per device.

v0:
```python
import functools

import jax
import jax.numpy as jnp
from jax import lax
from jax.experimental import pallas as pl
from jax.experimental.pallas import tpu as pltpu
from jax.sharding import PartitionSpec as P

SPAN = 64
MESH = pl.DeviceIdType.MESH


PRECISION_LEVEL = lax.Precision.HIGH


def entering(value, axis, join, neutral, kept=None):
    count = lax.axis_size(axis)
    place = lax.axis_index(axis)
    ahead = count - 1 - place
    if kept is None:
        kept = lax.all_gather(value[0].astype(jnp.bfloat16), axis)
    gathered = (kept, lax.all_gather(value[1].astype(jnp.bfloat16), axis))
    state = jax.tree.map(lambda a, e: jnp.zeros_like(a) + jnp.asarray(e, a.dtype), value, neutral)

    def one(lap, state):
        source = count - 1 - lap
        return join(
            state,
            jax.tree.map(
                lambda a, own: lax.dynamic_index_in_dim(a, source, 0, False).astype(own.dtype),
                gathered,
                value,
            ),
        )

    return lax.fori_loop(0, ahead, one, state)


def prefix(value, axis, join, neutral):
    count, mine = (lax.axis_size(axis), lax.axis_index(axis))
    pieces = lax.all_gather(value, axis)
    pieces = pieces[::-1]
    mine = count - 1 - mine
    subtotal = jnp.full_like(value, 0) + jnp.asarray(neutral, value.dtype)

    def lap(position, subtotal):
        longer = join(subtotal, pieces[position])
        return jnp.where(position < mine, longer, subtotal)

    return lax.fori_loop(0, count - 1, lap, subtotal)


def route_tables(routes, route_weights, experts, capacity):
    tokens = routes.shape[0]
    top_count = routes.shape[1]
    pair_ids = routes.reshape(-1)
    expert_ids = jnp.arange(experts, dtype=jnp.int32)
    onehot = (pair_ids[:, None] == expert_ids[None, :]).astype(jnp.int32)
    slot_rank = jnp.sum((jnp.cumsum(onehot, axis=0) - onehot) * onehot, axis=1)
    target = pair_ids * capacity + slot_rank
    slot_ids = jnp.arange(experts * capacity, dtype=jnp.int32)
    slot_hits = (
        (target[:, None] == slot_ids[None, :])
        .astype(jnp.float32)
        .reshape(tokens, top_count, experts * capacity)
    )
    placed = jnp.sum(slot_hits, axis=1)
    weighted = jnp.einsum("tk,tkp->tp", route_weights, slot_hits, precision=PRECISION_LEVEL)
    return (placed, weighted)


def expert_backward(inputs, pair_grad, gate_proj, up_proj, down_proj):
    gate_pre = jnp.einsum("erd,edf->erf", inputs, gate_proj, preferred_element_type=jnp.float32)
    up_pre = jnp.einsum("erd,edf->erf", inputs, up_proj, preferred_element_type=jnp.float32)
    sigmoid_gate = jax.nn.sigmoid(gate_pre)
    activated = gate_pre * sigmoid_gate
    hidden = (activated * up_pre).astype(jnp.bfloat16)
    down_grad = jnp.einsum("erf,erd->efd", hidden, pair_grad, preferred_element_type=jnp.float32)
    hidden_grad = jnp.einsum(
        "erd,efd->erf", pair_grad, down_proj, preferred_element_type=jnp.float32
    )
    gate_delta = (
        hidden_grad * up_pre * sigmoid_gate * (1.0 + gate_pre * (1.0 - sigmoid_gate))
    ).astype(jnp.bfloat16)
    up_delta = (hidden_grad * activated).astype(jnp.bfloat16)
    gate_grad = jnp.einsum("erd,erf->edf", inputs, gate_delta, preferred_element_type=jnp.float32)
    up_grad = jnp.einsum("erd,erf->edf", inputs, up_delta, preferred_element_type=jnp.float32)
    return (gate_grad, up_grad, down_grad, gate_delta, up_delta)


def input_rows(gate_delta, up_delta, gate_weight, up_weight):
    input_grad = jnp.einsum(
        "erf,edf->erd", gate_delta, gate_weight, preferred_element_type=jnp.float32
    )
    return input_grad + jnp.einsum(
        "erf,edf->erd", up_delta, up_weight, preferred_element_type=jnp.float32
    )


def state_combine(prior_steps, later):
    return (prior_steps[0] * later[0], later[1] + later[0][:, :, None] * prior_steps[1])


def add_combine(prior_steps, later):
    return prior_steps + later


def mixer_backward(queries, key_rows, value_rows, log_decay, entry, mix_grad, kept=None):
    tokens = queries.shape[0]
    heads = entry.shape[0]
    key_width = entry.shape[1]
    value_width = entry.shape[2]
    blocks = tokens // SPAN
    causal = jnp.tril(jnp.ones((SPAN, SPAN), dtype=bool))

    def split(rows, width):
        return rows.astype(jnp.float32).reshape(blocks, SPAN, heads, width)

    scaled_q = split(queries, key_width) * key_width ** (-0.5)
    key_segment = split(key_rows, key_width)
    value_segment = split(value_rows, value_width)
    decays = split(log_decay, key_width)
    output_gradient = split(mix_grad, value_width)
    value_dots = jnp.where(
        causal[None, None],
        jnp.einsum("nthv,nshv->nhts", output_gradient, value_segment, precision=PRECISION_LEVEL),
        0.0,
    )

    def forward_block(passed_state, block_data):
        query_now, current_key, current_value, decay_now, current_gradient, dots_now = block_data
        running_decay = jnp.cumsum(decay_now, axis=0)
        growth_multiplier = jnp.exp(running_decay)
        block_overall_sum = running_decay[-1]
        state_contribution = growth_multiplier * jnp.einsum(
            "gxb,xqb->gxq", current_gradient, passed_state, precision=PRECISION_LEVEL
        )
        inside = growth_multiplier * jnp.einsum(
            "hts,shk->thk",
            dots_now,
            current_key * jnp.exp(-running_decay),
            precision=PRECISION_LEVEL,
        )
        state_update = jnp.einsum(
            "rsx,rse->sxe",
            current_key * jnp.exp(block_overall_sum - running_decay),
            current_value,
            precision=PRECISION_LEVEL,
        )
        return (
            jnp.exp(block_overall_sum)[:, :, None] * passed_state + state_update,
            state_contribution + inside,
        )

    def reverse_block(passed_state, block_data):
        query_now, current_key, current_value, decay_now, current_gradient, dots_now = block_data
        running_decay = jnp.cumsum(decay_now, axis=0)
        shrink = jnp.exp(-running_decay)
        block_overall_sum = running_decay[-1]
        decay_remaining = jnp.exp(block_overall_sum - running_decay)
        query_raised = query_now * jnp.exp(running_decay)
        key_portion = decay_remaining * jnp.einsum(
            "gxb,xqb->gxq", current_value, passed_state, precision=PRECISION_LEVEL
        )
        key_portion = key_portion + shrink * jnp.einsum(
            "hts,thk->shk", dots_now, query_raised, precision=PRECISION_LEVEL
        )
        scores = jnp.where(
            causal[None],
            jnp.einsum(
                "thk,shk->hts", query_raised, current_key * shrink, precision=PRECISION_LEVEL
            ),
            0.0,
        )
        value_portion = jnp.einsum(
            "qgy,gye->qge", current_key * decay_remaining, passed_state, precision=PRECISION_LEVEL
        )
        value_portion = value_portion + jnp.einsum(
            "hts,thv->shv", scores, current_gradient, precision=PRECISION_LEVEL
        )
        prior_steps = (
            jnp.einsum("rsx,rse->sxe", query_raised, current_gradient, precision=PRECISION_LEVEL)
            + jnp.exp(block_overall_sum)[:, :, None] * passed_state
        )
        return (prior_steps, (key_portion, value_portion))

    block_inputs = (scaled_q, key_segment, value_segment, decays, output_gradient, value_dots)
    _, query_part = lax.scan(forward_block, entry, block_inputs)
    empty_state = jnp.zeros((heads, key_width, value_width), dtype=jnp.float32)
    local_start, (key_portion, value_portion) = lax.scan(
        reverse_block, empty_state, block_inputs, reverse=True
    )
    scaled_flat = scaled_q.reshape(tokens, heads, key_width)
    key_flattened = key_segment.reshape(tokens, heads, key_width)
    value_flattened = value_segment.reshape(tokens, heads, value_width)
    query_flat = query_part.reshape(tokens, heads, key_width)
    local_key = key_portion.reshape(tokens, heads, key_width)
    running_decay = jnp.cumsum(decays.reshape(tokens, heads, key_width), axis=0)
    device_total = running_decay[-1]
    decay_remaining = jnp.exp(device_total - running_decay)
    retain = jnp.exp(device_total)
    ones_head = jnp.ones((heads, key_width), dtype=jnp.float32)
    zeros_head = jnp.zeros((heads, key_width), dtype=jnp.float32)
    scanned = entering((retain, local_start), "sp", state_combine, (ones_head, empty_state), kept)
    following_state = scanned[1]
    key_full = local_key + decay_remaining * jnp.einsum(
        "gxb,xqb->gxq", value_flattened, following_state, precision=PRECISION_LEVEL
    )
    value_full = value_portion.reshape(tokens, heads, value_width)
    value_full = value_full + jnp.einsum(
        "qgy,gye->qge", key_flattened * decay_remaining, following_state, precision=PRECISION_LEVEL
    )
    change = scaled_flat * query_flat - key_flattened * key_full
    later_sum = prefix(jnp.sum(change, axis=0), "sp", add_combine, zeros_head)
    decay_grad = (lax.cumsum(change, axis=0, reverse=True) + later_sum[None]).reshape(
        tokens, heads * key_width
    )
    query_grad = (
        (query_flat * key_width ** (-0.5)).reshape(tokens, heads * key_width).astype(jnp.bfloat16)
    )
    key_grad = key_full.reshape(tokens, heads * key_width).astype(jnp.bfloat16)
    value_grad = value_full.reshape(tokens, heads * value_width).astype(jnp.bfloat16)
    return (query_grad, key_grad, value_grad, decay_grad)


def peers(nz):
    s = lax.axis_index("sp")
    t = lax.axis_index("tp")
    y, x = s // 2, s % 2
    z, c = t // 2, t % 2
    return s, (1 - y) * 2 + x, y * 2 + 1 - x, (1 - y) * 2 + 1 - x, z, c


def greet(devices):
    barrier = pltpu.get_barrier_semaphore()
    for device in devices:
        pl.semaphore_signal(barrier, inc=1, device_id=device, device_id_type=MESH)
    pl.semaphore_wait(barrier, len(devices))


def at(s, t):
    return {"sp": s, "tp": t}


def gather_kernel(
    nz,
    x_ref,
    g_ref,
    w_ref,
    wg_ref,
    wu_ref,
    xo,
    go,
    wo,
    wgo,
    wuo,
    z_send,
    z_recv,
    p_send,
    p_recv,
    d_send,
    d_recv,
    w_send,
    w_recv,
    t_send,
    t_recv,
    own_sem,
):
    s, sy, sx, sd, z, c = peers(nz)
    me, partner = z * 2 + c, z * 2 + 1 - c
    greet(
        [at(s, lax.rem(z + d, nz) * 2 + c) for d in range(1, nz)]
        + [at(sy, me), at(sx, me), at(sd, me), at(s, partner)]
    )
    sources, outs = (x_ref, g_ref), (xo, go)
    first, second = (sy, sx), (sx, sy)
    sent = []

    def copy(src, dst, send, recv, device):
        return pltpu.make_async_remote_copy(
            src_ref=src, dst_ref=dst, send_sem=send, recv_sem=recv, device_id=device, device_id_type=MESH
        )

    def start(*parts):
        made = copy(*parts)
        made.start()
        sent.append(made)

    def column(k):
        return lax.rem(z + k, nz) * 2 + c

    def source(a, k):
        return sources[a] if k == 0 else outs[a].at[s, column(k)]

    def plane(a, k, j, src, row, target):
        start(
            src,
            outs[a].at[row, column(k)],
            p_send.at[a, k, j],
            p_recv.at[a, k, j],
            at(target, me),
        )

    def arrived(a, k, j, row):
        slot = outs[a].at[row, column(k)]
        copy(slot, slot, p_send.at[a, k, j], p_recv.at[a, k, j], at(s, partner)).wait_recv()
        return slot

    def across(a, k, j, src, row):
        start(
            src,
            outs[a].at[row, column(k)],
            d_send.at[a, k, j],
            d_recv.at[a, k, j],
            at(s, partner),
        )

    def open_step(k):
        if k:
            for a in range(2):
                slot = outs[a].at[s, column(k)]
                copy(slot, slot, z_send.at[a, k - 1], z_recv.at[a, k - 1], at(s, partner)).wait_recv()
        for a in range(2):
            plane(a, k, 0, source(a, k), s, first[a])
        for a in range(2):
            plane(a, k, 1, source(a, k), s, second[a])
        for a in range(2):
            across(a, k, 0, source(a, k), s)

    def middle_step(k):
        for a in range(2):
            slot = arrived(a, k, 0, first[a])
            plane(a, k, 2, slot, first[a], second[a])
            across(a, k, 1, slot, first[a])

    def close_step(k):
        for a in range(2):
            across(a, k, 2, arrived(a, k, 1, second[a]), second[a])
        for a in range(2):
            across(a, k, 3, arrived(a, k, 2, sd), sd)

    for j, target in enumerate((sy, sx, sd)):
        start(w_ref, wo.at[s], w_send.at[j], w_recv.at[j], at(target, me))
    open_step(0)
    for d in range(1, nz):
        for a in range(2):
            start(
                sources[a],
                outs[a].at[s, me],
                z_send.at[a, d - 1],
                z_recv.at[a, d - 1],
                at(s, lax.rem(z + nz - d, nz) * 2 + c),
            )
    local = [
        pltpu.make_async_copy(x_ref, xo.at[s, me], own_sem.at[0]),
        pltpu.make_async_copy(g_ref, go.at[s, me], own_sem.at[1]),
        pltpu.make_async_copy(w_ref, wo.at[s], own_sem.at[2]),
    ]
    for one in local:
        one.start()
    for k in range(nz):
        for i, (src, dst) in enumerate(((wg_ref, wgo), (wu_ref, wuo))):
            start(src.at[k, 1 - c], dst.at[k], t_send.at[i, k], t_recv.at[i, k], at(s, partner))
    middle_step(0)
    for k in range(1, nz):
        open_step(k)
        close_step(k - 1)
        middle_step(k)
    close_step(nz - 1)
    for j, row in enumerate((sy, sx, sd)):
        slot = wo.at[row]
        copy(slot, slot, w_send.at[j], w_recv.at[j], at(s, partner)).wait_recv()
    for k in range(nz):
        for i, dst in enumerate((wgo, wuo)):
            slot = dst.at[k]
            copy(slot, slot, t_send.at[i, k], t_recv.at[i, k], at(s, partner)).wait_recv()
        for a in range(2):
            for j, row in enumerate((s, first[a], second[a], sd)):
                slot = outs[a].at[row, lax.rem(z + k, nz) * 2 + 1 - c]
                copy(slot, slot, d_send.at[a, k, j], d_recv.at[a, k, j], at(s, partner)).wait_recv()
    for one in sent:
        one.wait_send()
    for one in local:
        one.wait()


def gather_all(layer_input, out_cotangent, table, gate_rows, up_rows):
    nz = gate_rows.shape[0]
    rows, columns = layer_input.shape
    n_sp = lax.axis_size("sp")
    dma = pltpu.SemaphoreType.DMA
    vmem = pl.BlockSpec(memory_space=pltpu.VMEM)
    anywhere = pl.BlockSpec(memory_space=pl.ANY)
    tokens = jax.ShapeDtypeStruct((n_sp, 2 * nz, rows, columns), layer_input.dtype)
    halves = jax.ShapeDtypeStruct((nz,) + gate_rows.shape[2:], gate_rows.dtype)
    return pl.pallas_call(
        functools.partial(gather_kernel, nz),
        out_shape=(
            tokens,
            tokens,
            jax.ShapeDtypeStruct((n_sp,) + table.shape, table.dtype),
            halves,
            halves,
        ),
        in_specs=[vmem, vmem, vmem, anywhere, anywhere],
        out_specs=(anywhere,) * 5,
        scratch_shapes=[
            dma((2, nz - 1)),
            dma((2, nz - 1)),
            dma((2, nz, 3)),
            dma((2, nz, 3)),
            dma((2, nz, 4)),
            dma((2, nz, 4)),
            dma((3,)),
            dma((3,)),
            dma((2, nz)),
            dma((2, nz)),
            dma((3,)),
        ],
        compiler_params=pltpu.CompilerParams(collective_id=0, has_side_effects=True),
        name="gather_all",
    )(layer_input, out_cotangent, table, gate_rows, up_rows)


def dots(left, right, left_dim, right_dim):
    return lax.dot_general(
        left, right, (((left_dim,), (right_dim,)), ((), ())), preferred_element_type=jnp.float32
    )


def hidden_kernel(
    x_ref, g_ref, w_ref, wg_ref, wu_ref, wd_ref, gd, ud, gdt, udt, ht, gate, up, back
):
    step = pl.program_id(0)
    rows = gate.shape[0]
    columns = x_ref.shape[-1]

    @pl.when(step == 0)
    def _():
        for total in (gate, up, back):
            total[...] = jnp.zeros_like(total)

    x = x_ref[...].reshape(rows, columns)
    pair = (w_ref[...] * g_ref[...].reshape(rows, columns).astype(jnp.float32)).astype(jnp.bfloat16)
    gate[...] += dots(x, wg_ref[...], 1, 0)
    up[...] += dots(x, wu_ref[...], 1, 0)
    back[...] += dots(pair, wd_ref[...], 1, 1)

    @pl.when(step == pl.num_programs(0) - 1)
    def _():
        gate_pre, up_pre, grad = gate[...], up[...], back[...]
        sigmoid_gate = jax.nn.sigmoid(gate_pre)
        activated = gate_pre * sigmoid_gate
        gate_delta = grad * up_pre * sigmoid_gate * (1.0 + gate_pre * (1.0 - sigmoid_gate))
        up_delta = grad * activated
        gd[...] = gate_delta.astype(jnp.bfloat16)
        ud[...] = up_delta.astype(jnp.bfloat16)
        gdt[...] = gate_delta.T.astype(jnp.bfloat16)
        udt[...] = up_delta.T.astype(jnp.bfloat16)
        ht[...] = (activated * up_pre).T.astype(jnp.bfloat16)


def token_spec(tokens):
    return pl.BlockSpec((tokens.shape[0], 1) + tokens.shape[2:], lambda t: (0, t, 0, 0))


def fixed_spec(shape):
    return pl.BlockSpec(shape, lambda t: (0,) * len(shape))


def hidden_deltas(x, g, weight, gate_w, up_w, down_w):
    n_sp, tp, rows, columns = x.shape
    total, hidden = n_sp * rows, gate_w.shape[1]
    tall = jax.ShapeDtypeStruct((total, hidden), jnp.bfloat16)
    wide = jax.ShapeDtypeStruct((hidden, total), jnp.bfloat16)
    down_spec = pl.BlockSpec((hidden, columns), lambda t: (0, t))
    row_spec = pl.BlockSpec((columns, hidden), lambda t: (t, 0))
    return pl.pallas_call(
        hidden_kernel,
        grid=(tp,),
        out_shape=(tall, tall, wide, wide, wide),
        in_specs=[token_spec(x), token_spec(g), fixed_spec((total, 1)), row_spec, row_spec, down_spec],
        out_specs=[fixed_spec(tall.shape)] * 2 + [fixed_spec(wide.shape)] * 3,
        scratch_shapes=[pltpu.VMEM((total, hidden), jnp.float32)] * 3,
        cost_estimate=pl.CostEstimate(
            flops=6 * total * hidden * tp * columns, bytes_accessed=4 * x.size, transcendentals=0
        ),
        name="hidden_deltas",
    )(x, g, weight, gate_w, up_w, down_w)


def weight_kernel(x_ref, g_ref, w_ref, gdt, udt, ht, gate_out, up_out, down_out):
    rows = w_ref.shape[0]
    columns = x_ref.shape[-1]
    x = x_ref[...].reshape(rows, columns)
    pair = (w_ref[...] * g_ref[...].reshape(rows, columns).astype(jnp.float32)).astype(jnp.bfloat16)
    gate_out[...] = dots(gdt[...], x, 1, 0).T.astype(jnp.bfloat16)
    up_out[...] = dots(udt[...], x, 1, 0).T.astype(jnp.bfloat16)
    down_out[...] = dots(ht[...], pair, 1, 0).astype(jnp.bfloat16)


def weight_grads(x, g, weight, gdt, udt, ht):
    n_sp, tp, rows, columns = x.shape
    total, hidden = n_sp * rows, gdt.shape[0]
    tall = jax.ShapeDtypeStruct((tp * columns, hidden), jnp.bfloat16)
    wide = jax.ShapeDtypeStruct((hidden, tp * columns), jnp.bfloat16)
    row_spec = pl.BlockSpec((columns, hidden), lambda t: (t, 0))
    return pl.pallas_call(
        weight_kernel,
        grid=(tp,),
        out_shape=(tall, tall, wide),
        in_specs=[token_spec(x), token_spec(g), fixed_spec((total, 1))] + [fixed_spec(gdt.shape)] * 3,
        out_specs=[row_spec, row_spec, pl.BlockSpec((hidden, columns), lambda t: (0, t))],
        cost_estimate=pl.CostEstimate(
            flops=6 * total * hidden * tp * columns, bytes_accessed=4 * x.size, transcendentals=0
        ),
        name="weight_grads",
    )(x, g, weight, gdt, udt, ht)


def reduce_kernel(
    nz,
    gd,
    ud,
    wg,
    wu,
    wgp,
    wup,
    g_ref,
    out,
    other,
    s1,
    r1,
    keep,
    s2,
    r2,
    zs,
    zr,
    o_send,
    o_recv,
    a_send,
    a_recv,
    b_send,
    b_recv,
    z_send,
    z_recv,
):
    s, sy, sx, sd, z, c = peers(nz)
    me, partner = z * 2 + c, z * 2 + 1 - c
    rows = g_ref.shape[0]
    half = rows // 2
    greet(
        [at(s, lax.rem(z + d, nz) * 2 + c) for d in range(1, nz)]
        + [at(sy, me), at(sx, me), at(s, partner)]
    )
    sent = []

    def start(src, dst, send, recv, device):
        made = pltpu.make_async_remote_copy(
            src_ref=src, dst_ref=dst, send_sem=send, recv_sem=recv, device_id=device, device_id_type=MESH
        )
        made.start()
        sent.append(made)
        return made

    swaps = [
        start(ref, other.at[i], o_send.at[i], o_recv.at[i], at(s, partner))
        for i, ref in enumerate((gd, ud))
    ]
    for one in swaps:
        one.wait_recv()
    first, second = (sy, sx), (sx, sy)
    outgoing, crossing, final = {}, {}, {}

    def compute(k):
        column = lax.rem(z + nz - k, nz)
        weights = (wg[column, c], wu[column, c], wgp[column], wup[column])
        for i, q in enumerate((s, sy, sx, sd)):
            span = pl.ds(pl.multiple_of(q * rows, rows), rows)
            lefts = (gd[span, :], ud[span, :], other[0, span, :], other[1, span, :])
            tile = dots(lefts[0], weights[0], 1, 1)
            for left, weight in zip(lefts[1:], weights[1:]):
                tile = tile + dots(left, weight, 1, 1)
            for a in range(2):
                part = tile[a * half : (a + 1) * half]
                if i == 0:
                    keep[k, a, 0] = part
                elif i == 3:
                    s1[k, a, 1] = part.astype(jnp.bfloat16)
                elif i == 1 + a:
                    s1[k, a, 0] = part.astype(jnp.bfloat16)
                else:
                    keep[k, a, 1] = part
        for a in range(2):
            outgoing[k, a] = start(
                s1.at[k, a], r1.at[k, a], a_send.at[k, a], a_recv.at[k, a], at(first[a], me)
            )

    def middle(k):
        for a in range(2):
            outgoing[k, a].wait_recv()
            s2[k, a] = (keep[k, a, 1] + r1[k, a, 1].astype(jnp.float32)).astype(jnp.bfloat16)
            crossing[k, a] = start(
                s2.at[k, a], r2.at[k, a], b_send.at[k, a], b_recv.at[k, a], at(second[a], me)
            )

    def close(k):
        for a in range(2):
            crossing[k, a].wait_recv()
            total = (
                keep[k, a, 0]
                + r1[k, a, 0].astype(jnp.float32)
                + r2[k, a].astype(jnp.float32)
            )
            if k:
                zs[k - 1, a * half : (a + 1) * half] = total.astype(jnp.bfloat16)
            else:
                keep[k, a, 0] = total
        if k:
            final[k] = start(
                zs.at[k - 1],
                zr.at[k - 1],
                z_send.at[k - 1],
                z_recv.at[k - 1],
                at(s, lax.rem(z + nz - k, nz) * 2 + c),
            )

    order = list(range(1, nz)) + [0]
    for i in range(nz + 2):
        if i < nz:
            compute(order[i])
        if 0 <= i - 2 < nz:
            close(order[i - 2])
        if 0 <= i - 1 < nz:
            middle(order[i - 1])
    for k in range(1, nz):
        final[k].wait_recv()
    for a in range(2):
        span = slice(a * half, (a + 1) * half)
        total = keep[0, a, 0]
        for k in range(1, nz):
            total = total + zr[k - 1, span].astype(jnp.float32)
        out[span] = (g_ref[span].astype(jnp.float32) + total).astype(jnp.bfloat16)
    for one in sent:
        one.wait_send()


def reduce_all(gd, ud, gate_rows, up_rows, gate_other, up_other, out_cotangent):
    nz = gate_rows.shape[0]
    rows, columns = out_cotangent.shape
    half = rows // 2
    dma = pltpu.SemaphoreType.DMA
    vmem = pl.BlockSpec(memory_space=pltpu.VMEM)
    bf16 = jnp.bfloat16
    return pl.pallas_call(
        functools.partial(reduce_kernel, nz),
        out_shape=jax.ShapeDtypeStruct((rows, columns), bf16),
        in_specs=[vmem] * 7,
        out_specs=vmem,
        scratch_shapes=[
            pltpu.VMEM((2,) + gd.shape, bf16),
            pltpu.VMEM((nz, 2, 2, half, columns), bf16),
            pltpu.VMEM((nz, 2, 2, half, columns), bf16),
            pltpu.VMEM((nz, 2, 2, half, columns), jnp.float32),
            pltpu.VMEM((nz, 2, half, columns), bf16),
            pltpu.VMEM((nz, 2, half, columns), bf16),
            pltpu.VMEM((nz - 1, rows, columns), bf16),
            pltpu.VMEM((nz - 1, rows, columns), bf16),
            dma((2,)),
            dma((2,)),
            dma((nz, 2)),
            dma((nz, 2)),
            dma((nz, 2)),
            dma((nz, 2)),
            dma((nz - 1,)),
            dma((nz - 1,)),
        ],
        compiler_params=pltpu.CompilerParams(collective_id=1, has_side_effects=True),
        name="reduce_all",
    )(gd, ud, gate_rows, up_rows, gate_other, up_other, out_cotangent)


def dense_experts(layer_input, out_cotangent, routes, route_weights, gate_proj, up_proj, down_proj, log_decay):
    n_sp, tp = lax.axis_size("sp"), lax.axis_size("tp")
    nz = tp // 2
    columns = layer_input.shape[1]
    hidden = gate_proj.shape[2]
    rows = [
        jnp.sum(jnp.where(routes == e, route_weights, 0.0), axis=1) for e in range(n_sp)
    ] + [jnp.exp(jnp.sum(log_decay, axis=0))]
    table = jnp.pad(jnp.stack(rows), ((0, -len(rows) % 8), (0, 0)))
    gate_rows = gate_proj.reshape(nz, 2, columns, hidden)
    up_rows = up_proj.reshape(nz, 2, columns, hidden)
    x, g, tables, gate_other, up_other = gather_all(
        layer_input, out_cotangent, table, gate_rows, up_rows
    )
    weight = lax.dynamic_index_in_dim(tables, lax.axis_index("sp"), 1, False).reshape(-1, 1)
    gd, ud, gdt, udt, ht = hidden_deltas(x, g, weight, gate_proj[0], up_proj[0], down_proj[0])
    token_grad = reduce_all(gd, ud, gate_rows, up_rows, gate_other, up_other, out_cotangent)
    grads = weight_grads(x, g, weight, gdt, udt, ht)
    return [part[None] for part in grads], token_grad, tables[:, n_sp]


def routed_experts(
    layer_input, out_cotangent, routes, route_weights, gate_proj, up_proj, down_proj
):
    experts = gate_proj.shape[0] * lax.axis_size("sp")
    capacity = 5 * routes.shape[1] * routes.shape[0] // (4 * experts)
    columns = layer_input.shape[1]
    placed, weighted = route_tables(routes, route_weights, experts, capacity)
    input_slots = (
        jnp.einsum(
            "tp,td->pd",
            placed.astype(jnp.bfloat16),
            layer_input,
            preferred_element_type=jnp.float32,
        )
        .astype(jnp.bfloat16)
        .reshape(experts, capacity, columns)
    )
    grad_slots = (
        jnp.einsum(
            "tp,td->pd", weighted, out_cotangent.astype(jnp.float32), precision=PRECISION_LEVEL
        )
        .astype(jnp.bfloat16)
        .reshape(experts, capacity, columns)
    )
    sent = (
        lax.all_to_all(input_slots, "sp", split_axis=0, concat_axis=1, tiled=True),
        lax.all_to_all(grad_slots, "sp", split_axis=0, concat_axis=1, tiled=True),
    )
    inputs = lax.all_gather(sent[0], "tp", axis=2, tiled=True)
    pair_grad = lax.all_gather(sent[1], "tp", axis=2, tiled=True)
    gate_part, up_part, down_part, gate_delta, up_delta = expert_backward(
        inputs, pair_grad, gate_proj, up_proj, down_proj
    )
    input_grad = input_rows(gate_delta, up_delta, gate_proj, up_proj)
    share = lax.psum_scatter(
        input_grad.astype(jnp.bfloat16), "tp", scatter_dimension=2, tiled=True
    ).astype(jnp.float32)
    returned = lax.all_to_all(
        share.astype(jnp.bfloat16), "sp", split_axis=1, concat_axis=0, tiled=True
    ).astype(share.dtype)
    slot_grads = returned.reshape(experts * capacity, columns)
    moe_grad = jnp.einsum("tp,pd->td", placed, slot_grads, precision=PRECISION_LEVEL)
    token_grad = (out_cotangent.astype(jnp.float32) + moe_grad).astype(jnp.bfloat16)
    parts = [part.astype(jnp.bfloat16) for part in (gate_part, up_part, down_part)]
    return parts, token_grad, None


def body(
    layer_input,
    out_cotangent,
    routes,
    route_weights,
    gate_proj,
    up_proj,
    down_proj,
    out_proj,
    mixer_output,
    queries,
    key_rows,
    value_rows,
    log_decay,
    entry_state,
):
    args = (layer_input, out_cotangent, routes, route_weights, gate_proj, up_proj, down_proj)
    paired = lax.axis_size("sp") == 4 and lax.axis_size("tp") % 2 == 0
    if paired and gate_proj.shape[0] == 1 and log_decay.shape[1] == routes.shape[0]:
        parts, token_grad, kept = dense_experts(*args, log_decay)
        kept = kept.reshape(kept.shape[0], *entry_state.shape[1:3])
    else:
        parts, token_grad, kept = routed_experts(*args)
    full_grad = lax.all_gather(token_grad, "tp", axis=1, tiled=True)
    partial = jnp.einsum(
        "td,tc->dc", full_grad, mixer_output, preferred_element_type=jnp.float32
    ).astype(jnp.bfloat16)
    partial, full_grad = lax.optimization_barrier((partial, full_grad))
    proj_grad = lax.psum_scatter(partial, "sp", scatter_dimension=0, tiled=True).astype(jnp.float32)
    mix_grad = jnp.dot(full_grad, out_proj, preferred_element_type=jnp.float32).astype(jnp.bfloat16)
    query_grad, key_grad, value_grad, decay_grad = mixer_backward(
        queries, key_rows, value_rows, log_decay, entry_state[0], mix_grad, kept
    )
    return (
        *parts,
        proj_grad,
        query_grad,
        key_grad,
        value_grad,
        decay_grad,
    )


def solution(mesh):
    return jax.shard_map(
        body,
        mesh=mesh,
        in_specs=(
            P("sp", "tp"),
            P("sp", "tp"),
            P("sp", None),
            P("sp", None),
            P("sp", None, "tp"),
            P("sp", None, "tp"),
            P("sp", "tp", None),
            P(None, "tp"),
            P("sp", "tp"),
            P("sp", "tp"),
            P("sp", "tp"),
            P("sp", "tp"),
            P("sp", "tp"),
            P("sp", "tp", None, None),
        ),
        out_specs=(
            P("sp", None, "tp"),
            P("sp", None, "tp"),
            P("sp", "tp", None),
            P("sp", "tp"),
            P("sp", "tp"),
            P("sp", "tp"),
            P("sp", "tp"),
            P("sp", "tp"),
        ),
        check_vma=False,
    )
```

profile of v0, /device:TPU:0, one launch (start us, length us, event | category | flops | bytes accessed | tf_op | source)
XLA Modules:
  0.0 293.2 jit_solution(11594331258060295122)
XLA Ops:
  7.2 1.0 reduce_sum.58
  8.3 0.7 fusion.76
  9.0 0.6 pad.4.w_ref
  9.6 90.7 %gather_all.1 = (bf16[4,8,256,512]{3,2,1,0:T(8,128)(2,1)}, bf16[4,8,256,512]{3,2,1,0:T(8,128)(2,1)}, f32[4,8,256]{2,1,0:T(8,128)}, bf16[4,512,256]{2,1,0:T(8,128)(2,1)}, bf16[4,512,256]{2,1,0:T(8,128)(2,1)}) custom-call(bf16[256,512]{1,0:T(8,128)(2,1)} %x_ref.1, bf16[256,512]{1,0:T(8,128)(2,1)} %g_ref.3, f32[8,256]{1,0:T(8,128)} %pad.4.w_ref, ...), custom_call_target="tpu_custom_call" | custom-call | tf_op jit(solution)/shard_map/gather_all/pallas_call | solution.py:397
  100.3 0.8 fusion.79
  101.2 1.0 copy.130.w_ref
  102.2 15.3 %hidden_deltas.1 = (bf16[1024,256]{1,0:T(8,128)(2,1)}, bf16[1024,256]{1,0:T(8,128)(2,1)}, bf16[256,1024]{1,0:T(8,128)(2,1)}, bf16[256,1024]{1,0:T(8,128)(2,1)}, bf16[256,1024]{1,0:T(8,128)(2,1)}) custom-call(bf16[4,8,256,512]{3,2,1,0:T(8,128)(2,1)} %get-tuple-element.447.x_ref, bf16[4,8,256,512]{3,2,1,0:T(8,128)(2,1)} %get-tuple-element.448.g_ref, ...), custom_call_target="tpu_custom_call" | custom-call | flops 6442450944 | bytes 16777216 | tf_op jit(solution)/shard_map/hidden_deltas/pallas_call | solution.py:479
  117.5 53.6 %reduce_all.1 = bf16[256,512]{1,0:T(8,128)(2,1)} custom-call(bf16[1024,256]{1,0:T(8,128)(2,1)} %get-tuple-element.456.gd, bf16[1024,256]{1,0:T(8,128)(2,1)} %get-tuple-element.457.ud, bf16[4,2,512,256]{3,2,1,0:T(8,128)(2,1)} %bitcast.255, bf16[4,2,512,256]{3,2,1,0:T(8,128)(2,1)} %bitcast.258, bf16[4,512,256]{2,1,0:T(8,128)(2,1)} %get-tuple-element.458.wgp, ...), custom_call_target="tpu_custom_call" | custom-call | tf_op jit(solution)/shard_map/reduce_all/pallas_call | solution.py:656
  171.7 0.8 mul.147
  172.6 0.8 copy.151
  174.9 13.8 %weight_grads.1 = (bf16[4096,256]{1,0:T(8,128)(2,1)}, bf16[4096,256]{1,0:T(8,128)(2,1)}, bf16[256,4096]{1,0:T(8,128)(2,1)}) custom-call(bf16[4,8,256,512]{3,2,1,0:T(8,128)(2,1)} %get-tuple-element.447.x_ref, bf16[4,8,256,512]{3,2,1,0:T(8,128)(2,1)} %get-tuple-element.448.g_ref, f32[1024,1]{1,0:T(8,128)} %copy.130.w_ref, ...), custom_call_target="tpu_custom_call" | custom-call | flops 6442450944 | bytes 16777216 | tf_op jit(solution)/shard_map/weight_grads/pallas_call | solution.py:509
  188.6 10.0 %all-gather.5.cloned.1.call-done = bf16[256,4096]{1,0:T(8,128)(2,1)} async-done(((bf16[256,512]{1,0:T(8,128)(2,1)}), bf16[256,4096]{1,0:T(8,128)(2,1)}) %all-gather.5.cloned.1.call-update) | async-done | bytes 2097168 | tf_op jit(solution)/shard_map/all_gather | solution.py:775
  198.6 4.8 %convolution_convert_fusion = bf16[4096,512]{1,0:T(8,128)(2,1)} fusion(bf16[256,4096]{1,0:T(8,128)(2,1)} %all-gather.5.cloned.1.call-done, bf16[256,512]{1,0:T(8,128)(2,1)S(1)} %copy-done), kind=kOutput, calls=%fused_computation.83 | convolution fusion | flops 1075838976 | bytes 6553600 | tf_op jit(solution)/shard_map/td,tc->dc/dot_general | solution.py:776
  203.4 4.1 %convolution_convert_fusion.1 = bf16[256,512]{1,0:T(8,128)(2,1)S(1)} fusion(bf16[256,4096]{1,0:T(8,128)(2,1)} %all-gather.5.cloned.1.call-done, bf16[4096,512]{1,0:T(8,128)(2,1)} %param.29), kind=kOutput, calls=%fused_computation.86 | convolution fusion | flops 1073872896 | bytes 6553600 | tf_op jit(solution)/shard_map/dot_general | solution.py:781
  207.6 0.9 convolution_select_fusion.1
  208.6 0.7 broadcast.23.clone
  209.3 16.0 %while.61 = (s32[]{:T(128)}, f32[2,128,256]{2,1,0:T(8,128)S(1)}, f32[4,64,2,128]{3,1,0,2:T(8,128)}, f32[4,64,2,256]{3,1,0,2:T(8,128)S(1)}, f32[4,64,2,128]{3,2,1...) while((s32[]{:T(128)}, f32[2,128,256]{2,1,0:T(8,128)S(1)}, ...), condition=%wide.region_11.12_spmd.clone, body=%wide.region_9.11_spmd.clone.sunk | while | flops 102232064 | bytes 3197089 | solution.py:191
  209.3 0.9 bitcast_multiply_fusion.6
  210.7 0.3 fusion.141
  211.0 0.3 fusion.139
  211.3 1.7 fusion.140
  213.0 0.3 convolution_add_fusion.5
  213.3 0.9 bitcast_multiply_fusion.6
  214.7 0.3 fusion.141
  215.0 0.3 fusion.139
  215.3 1.7 fusion.140
  217.0 0.3 convolution_add_fusion.5
  217.3 0.9 bitcast_multiply_fusion.6
  218.7 0.3 fusion.141
  219.0 0.3 fusion.139
  219.3 1.7 fusion.140
  221.0 0.3 convolution_add_fusion.5
  221.3 0.9 bitcast_multiply_fusion.6
  223.0 0.3 fusion.139
  223.3 1.7 fusion.140
  225.0 0.3 convolution_add_fusion.5
  225.4 1.8 copy.145
  227.2 0.9 copy-done.1
  228.1 9.6 %while.59 = (s32[]{:T(128)}, f32[2,128,256]{2,1,0:T(8,128)S(1)}, f32[4,64,2,128]{3,1,2,0:T(8,128)}, f32[4,64,2,128]{3,2,1,0:T(2,128)S(1)}, f32[4,64,2,128]{3,2,1...) while((s32[]{:T(128)}, f32[2,128,256]{2,1,0:T(8,128)S(1)}, ...), condition=%wide.region_8.9_spmd, body=%wide.region_6.8_spmd.sunk | while | flops 57884672 | bytes 1907821 | solution.py:189
  228.3 0.3 convolution_bitcast_fusion.10
  228.6 1.6 fusion.125
  230.2 0.3 convolution_add_fusion.4
  230.7 0.3 convolution_bitcast_fusion.10
  231.0 1.6 fusion.125
  232.6 0.3 convolution_add_fusion.4
  233.1 0.3 convolution_bitcast_fusion.10
  233.4 1.6 fusion.125
  235.0 0.3 convolution_add_fusion.4
  235.5 0.3 convolution_bitcast_fusion.10
  235.8 1.6 fusion.125
  237.4 0.3 convolution_add_fusion.4
  237.8 1.0 copy.152
  238.9 15.9 %all-gather = bf16[8,128,256]{2,1,0:T(8,128)(2,1)S(1)} all-gather(bf16[2,128,256]{2,1,0:T(8,128)(2,1)S(1)} %convert_element_type.57), channel_id=2, replica_groups=mesh['sp'=4,'tp'=8] {'sp'}, dimensions={0}, use_global_device_ids=true | all-gather | bytes 655360 | tf_op jit(solution)/shard_map/all_gather | solution.py:23
  254.9 0.5 while.60
  255.4 0.4 fusion.78
  256.2 2.2 fusion.80
  258.5 7.8 %all-gather.2 = f32[4,2,128]{2,1,0:T(2,128)S(1)} all-gather(f32[1,2,128]{2,1,0:T(2,128)S(1)} %bitcast.278), channel_id=3, replica_groups=mesh['sp'=4,'tp'=8] {'sp'}, dimensions={0}, use_global_device_ids=true | all-gather | bytes 5120 | tf_op jit(solution)/shard_map/all_gather | solution.py:42
  266.7 0.8 copy.159
  267.7 0.5 fusion.62
  268.2 0.8 copy.158
  269.0 0.8 copy.157
  270.0 0.7 copy.228
  270.6 12.9 %reduce-scatter.2.cloned.1.call-done = bf16[1024,512]{1,0:T(8,128)(2,1)} async-done(((bf16[4096,512]{1,0:T(8,128)(2,1)}), bf16[1024,512]{1,0:T(8,128)(2,1)}) %reduce-scatter.2.cloned.1.call-update) | async-done | bytes 1048592 | tf_op jit(solution)/shard_map/reduce_scatter | solution.py:780
  283.5 2.8 convert_element_type.51
  (115 shorter events, 6.6 us)
Async XLA Ops:
  7.2 191.4 %copy-start = (bf16[256,512]{1,0:T(8,128)(2,1)S(1)}, bf16[256,512]{1,0:T(8,128)(2,1)}, u32[]{:S(2)}) copy-start(bf16[256,512]{1,0:T(8,128)(2,1)} %param.30) | copy-start | bytes 786436
  7.2 191.4 %all-gather.5.cloned.1.call-start = ((), (), s32[]{:S(2)}) async-start(), calls=%async_computation.1 | async-start | bytes 2359296 | tf_op jit(solution)/shard_map/all_gather | solution.py:775
  117.5 53.9 %copy-start.2 = (f32[256,256]{1,0:T(8,128)S(1)}, f32[256,256]{1,0:T(8,128)}, u32[]{:S(2)}) copy-start(f32[256,256]{1,0:T(8,128)} %param.34) | copy-start | bytes 786436
  117.5 54.2 %copy-start.9 = (bf16[256,256]{1,0:T(8,128)(2,1)S(1)}, bf16[256,256]{1,0:T(8,128)(2,1)}, u32[]{:S(2)}) copy-start(bf16[256,256]{1,0:T(8,128)(2,1)} %param.31) | copy-start | bytes 393220
  171.1 2.3 copy-start.8
  171.1 2.5 copy-start.3
  171.1 112.4 %reduce-scatter.2.cloned.1.call-start = ((), (), s32[]{:S(2)}) async-start(), calls=%async_computation.2 | async-start | bytes 5242880 | tf_op jit(solution)/shard_map/reduce_scatter | solution.py:780
  227.2 0.9 copy-start.1
  238.9 16.5 %copy-start.4 = (bf16[256,512]{1,0:T(8,128)(2,1)S(1)}, bf16[256,512]{1,0:T(8,128)(2,1)}, u32[]{:S(2)}) copy-start(bf16[256,512]{1,0:T(8,128)(2,1)} %param.33) | copy-start | bytes 786436
  238.9 16.5 %copy-start.5 = (f32[256,256]{0,1:T(8,128)S(1)}, f32[256,256]{0,1:T(8,128)}, u32[]{:S(2)}) copy-start(f32[256,256]{0,1:T(8,128)} %copy.151) | copy-start | bytes 786436
  238.9 16.5 %copy-start.6 = (f32[256,2,128]{0,2,1:T(8,128)S(1)}, f32[256,2,128]{0,2,1:T(8,128)}, u32[]{:S(2)}) copy-start(f32[256,2,128]{0,2,1:T(8,128)} %copy.145) | copy-start | bytes 786436
  266.6 3.1 %copy-start.7 = (f32[4,64,2,128]{3,1,2,0:T(8,128)S(1)}, f32[4,64,2,128]{3,1,2,0:T(8,128)}, u32[]{:S(2)}) copy-start(f32[4,64,2,128]{3,1,2,0:T(8,128)} %get-tuple-element.462) | copy-start | bytes 786436
Sparse Core Ops, SparseCore 0:
  171.3 27.3 all-gather.4
  227.3 56.1 reduce-scatter.1
where the time goes:
time: 295 us; the launch traced here: 293 us
  Pallas kernels  173 us (59%)
  matrix products  31.5 us (11%)
  blocking collectives  23.8 us (8%)
  waiting for transfers between devices  22.9 us (8%)
  between operations  14.5 us (5%)
  local copies, waits for them, and re-layouts  14.3 us (5%)
  other arithmetic  12.1 us (4%)
    pallas_call x1, Pallas kernels, gather_all(): pl.pallas_call(functools.partial(gather_kernel, nz), out_shape=(tokens, t...  90.7 us
    pallas_call x1, Pallas kernels, reduce_all(): pl.pallas_call(functools.partial(reduce_kernel, nz), out_shape=jax.ShapeD...  53.6 us
    all_gather x1, blocking collectives, entering(): gathered = (kept, lax.all_gather(value[1].astype(jnp.bfloat16), axis))  15.9 us
    pallas_call x1, Pallas kernels, hidden_deltas(): pl.pallas_call(hidden_kernel, grid=(tp,), out_shape=(tall, tall, wide, wi...  15.3 us
    pallas_call x1, Pallas kernels, weight_grads(): pl.pallas_call(weight_kernel, grid=(tp,), out_shape=(tall, tall, wide), i...  13.8 us
    reduce_scatter x1, waiting for transfers between devices, body(): lax.psum_scatter(partial, 'sp', scatter_dimension=0, tiled=True)  12.9 us
    all_gather x1, waiting for transfers between devices, body(): full_grad = lax.all_gather(token_grad, 'tp', axis=1, tiled=True)  9.97 us
    all_gather x1, blocking collectives, prefix(): pieces = lax.all_gather(value, axis)  7.85 us
  transfers between devices with their start and end apart: 2, of which 2 were waited for; matrix products, arithmetic and copies ran while one was open for 7% of the time, Pallas kernels for 5%

commit v1 on v0

--- a/solution.py
+++ b/solution.py
@@ -681,6 +681,395 @@
     )(gd, ud, gate_rows, up_rows, gate_other, up_other, out_cotangent)
 
 
+def pieces(value):
+    if value.dtype == jnp.bfloat16:
+        return (value,)
+    high = value.astype(jnp.bfloat16)
+    return (high, (value - high.astype(jnp.float32)).astype(jnp.bfloat16))
+
+
+def product(left, right, left_dim, right_dim):
+    lefts, rights = pieces(left), pieces(right)
+    total = None
+    for i, one in enumerate(lefts):
+        for j, two in enumerate(rights):
+            if i + j < 2:
+                part = dots(one, two, left_dim, right_dim)
+                total = part if total is None else total + part
+    return total
+
+
+def exact(left, right):
+    return lax.dot_general(
+        left,
+        right,
+        (((1,), (0,)), ((), ())),
+        precision=lax.Precision.HIGHEST,
+        preferred_element_type=jnp.float32,
+    )
+
+
+def triangle(lower):
+    row = lax.broadcasted_iota(jnp.int32, (SPAN, SPAN), 0)
+    column = lax.broadcasted_iota(jnp.int32, (SPAN, SPAN), 1)
+    return row >= column if lower else row <= column
+
+
+def tail_kernel(
+    tg,
+    wo,
+    mo,
+    q_ref,
+    k_ref,
+    v_ref,
+    a_ref,
+    s0,
+    proj,
+    dq,
+    dk,
+    dv,
+    da,
+    full,
+    tgd,
+    moa,
+    mg,
+    gb,
+    grow,
+    shrink,
+    left,
+    raised,
+    kshrunk,
+    kleft,
+    scores,
+    states,
+    ends,
+    dqs,
+    dks,
+    dvs,
+    rout,
+    rin,
+    following,
+    kept_out,
+    kept_in,
+    sum_out,
+    sum_in,
+    z_send,
+    z_recv,
+    p_send,
+    p_recv,
+    b_send,
+    b_recv,
+    t_send,
+    t_recv,
+    m_send,
+    m_recv,
+    r_send,
+    r_recv,
+    k_send,
+    k_recv,
+    u_send,
+    u_recv,
+):
+    s, sy, sx, sd, z, c = peers(4)
+    nz = 4
+    me, partner = z * 2 + c, z * 2 + 1 - c
+    tokens, columns = tg.shape
+    blocks = tokens // SPAN
+    heads, width, span = s0.shape[0], s0.shape[1], s0.shape[2]
+    greet(
+        [at(s, lax.rem(z + d, nz) * 2 + c) for d in range(1, nz)]
+        + [at(sy, me), at(sx, me), at(sd, me), at(s, partner)]
+    )
+    sent = []
+
+    def copy(src, dst, send, recv, device):
+        return pltpu.make_async_remote_copy(
+            src_ref=src, dst_ref=dst, send_sem=send, recv_sem=recv, device_id=device, device_id_type=MESH
+        )
+
+    def start(when, *parts):
+        def go():
+            copy(*parts).start()
+
+        if when is None:
+            go()
+        else:
+            pl.when(when)(go)
+        sent.append((when, parts))
+
+    def arrived(slot, recv):
+        copy(slot, slot, recv, recv, at(s, partner)).wait_recv()
+
+    def slot(block, core):
+        return full.at[block * 2 + core]
+
+    def rows(index):
+        return pl.ds(pl.multiple_of(index * tokens, tokens), tokens)
+
+    def spread(when, src, block):
+        start(when, src, slot(block, c), b_send.at[block], b_recv.at[block], at(s, partner))
+        ok = block != s
+        start(
+            ok if when is None else when & ok,
+            src,
+            tgd.at[c, rows(s)],
+            p_send.at[block],
+            p_recv.at[s],
+            at(block, me),
+        )
+
+    def hop(when, src, block, way, d):
+        step = 1 if way == 0 else -1
+        room = z + step < nz if way == 0 else z + step >= 0
+        start(
+            room if when is None else when & room,
+            src,
+            slot(block, c),
+            z_send.at[way, d],
+            z_recv.at[way, d],
+            at(s, (z + step) * 2 + c),
+        )
+
+    hop(None, tg, z, 0, 0)
+    hop(None, tg, z, 1, 0)
+    spread(None, tg, z)
+    for j, target in enumerate((sy, sx, sd)):
+        start(None, mo, moa.at[rows(s)], m_send.at[j], m_recv.at[j], at(target, me))
+
+    lower, upper = triangle(True), triangle(False)
+    ones_low = lower.astype(jnp.float32)
+    scale = width ** (-0.5)
+    for n in range(blocks):
+        rn = slice(n * SPAN, (n + 1) * SPAN)
+        running = exact(ones_low, a_ref[rn, :])
+        end = running[SPAN - 1 : SPAN]
+        ends[n : n + 1, :] = end
+        kk = k_ref[rn, :].astype(jnp.float32)
+        up, down = jnp.exp(running), jnp.exp(-running)
+        rest = jnp.exp(end - running)
+        grow[rn, :] = up
+        shrink[rn, :] = down
+        left[rn, :] = rest
+        raised[rn, :] = q_ref[rn, :].astype(jnp.float32) * scale * up
+        kshrunk[rn, :] = kk * down
+        kleft[rn, :] = kk * rest
+    later = jnp.zeros((1, ends.shape[1]), jnp.float32)
+    laters = [None] * blocks
+    for n in reversed(range(blocks)):
+        laters[n] = later
+        later = later + ends[n : n + 1, :]
+    kept_out[...] = jnp.broadcast_to(jnp.exp(later), kept_out.shape)
+    for h in range(heads):
+        lk, lv = slice(h * width, (h + 1) * width), slice(h * span, (h + 1) * span)
+        state = s0[h].T
+        for n in range(blocks):
+            rn = slice(n * SPAN, (n + 1) * SPAN)
+            states[h, n] = state
+            score = product(kshrunk[rn, lk], raised[rn, lk], 1, 1)
+            scores[h, rn, :] = jnp.where(upper, score, 0.0)
+            if n + 1 < blocks:
+                state = jnp.exp(ends[n : n + 1, lk]) * state + product(v_ref[rn, lv], kleft[rn, lk], 0, 0)
+    for j in range(3):
+        start(
+            s > j, kept_out, kept_in.at[s], k_send.at[j], k_recv.at[s], at(j, me)
+        )
+
+    def mix(block, core, first=False):
+        index = block * 2 + core
+        part = dots(
+            tg[...] if first else full[index],
+            wo[pl.ds(pl.multiple_of(index * columns, columns), columns), :],
+            1,
+            0,
+        )
+        if first:
+            mg[...] = part
+        else:
+            mg[...] += part
+
+    mix(z, c, True)
+    full[me] = tg[...]
+    arrived(slot(z, 1 - c), b_recv.at[z])
+    mix(z, 1 - c)
+    for d in range(1, nz):
+        for way in range(2):
+            block = z - d if way == 0 else z + d
+            here = block >= 0 if way == 0 else block < nz
+
+            @pl.when(here)
+            def _():
+                arrived(slot(block, c), z_recv.at[way, d - 1])
+
+            if d < nz - 1:
+                hop(here, slot(block, c), block, way, d)
+            spread(here, slot(block, c), block)
+
+            @pl.when(here)
+            def _():
+                mix(block, c)
+                arrived(slot(block, 1 - c), b_recv.at[block])
+                mix(block, 1 - c)
+
+    gb[...] = mg[...].astype(jnp.bfloat16)
+
+    for h in range(heads):
+        lk, lv = slice(h * width, (h + 1) * width), slice(h * span, (h + 1) * span)
+        carry = jnp.zeros((span, width), jnp.float32)
+        for n in reversed(range(blocks)):
+            rn = slice(n * SPAN, (n + 1) * SPAN)
+            g, v = gb[rn, lv], v_ref[rn, lv]
+            down, over = jnp.where(lower, dots(g, v, 1, 1), 0.0), jnp.where(upper, dots(v, g, 1, 1), 0.0)
+            dqs[rn, lk] = grow[rn, lk] * (
+                product(g, states[h, n], 1, 0) + product(down, kshrunk[rn, lk], 1, 0)
+            )
+            kpart = shrink[rn, lk] * product(over, raised[rn, lk], 1, 0)
+            vpart = product(scores[h, rn, :], g, 1, 0)
+            if n + 1 < blocks:
+                kpart += left[rn, lk] * product(v, carry, 1, 0)
+                vpart += product(kleft[rn, lk], carry, 1, 1)
+            dks[rn, lk] = kpart
+            dvs[rn, lv] = vpart
+            carry = product(g, raised[rn, lk], 0, 0) + jnp.exp(ends[n : n + 1, lk]) * carry
+        rout[h] = carry.astype(jnp.bfloat16)
+        for j in range(3):
+            start(s > j, rout.at[h], rin.at[s, h], r_send.at[h, j], r_recv.at[h, s], at(j, me))
+
+    dq[...] = (dqs[...] * scale).astype(jnp.bfloat16)
+
+    for j, other in enumerate((sy, sx, sd)):
+        block = tgd.at[c, rows(other)]
+        arrived(block, p_recv.at[other])
+        start(None, block, block, t_send.at[j], t_recv.at[j], at(s, partner))
+        arrived(moa.at[rows(other)], m_recv.at[j])
+    moa[rows(s), :] = mo[...]
+    for core in range(2):
+        tgd[core, rows(s), :] = full[s * 2 + core]
+    for j, other in enumerate((sy, sx, sd)):
+        arrived(tgd.at[1 - c, rows(other)], t_recv.at[j])
+    for core in range(2):
+        proj[core * columns : (core + 1) * columns, :] = dots(tgd[core], moa[...], 0, 0)
+
+    following[...] = jnp.zeros_like(following)
+    for source in (3, 2, 1):
+
+        @pl.when(s < source)
+        def _():
+            arrived(kept_in.at[source], k_recv.at[source])
+            for h in range(heads):
+                arrived(rin.at[source, h], r_recv.at[h, source])
+                keep = kept_in[source, 0:1, h * width : (h + 1) * width]
+                following[h] = rin[source, h].astype(jnp.float32) + keep * following[h]
+
+    change = [None] * blocks
+    for n in reversed(range(blocks)):
+        rn = slice(n * SPAN, (n + 1) * SPAN)
+        rest = left[rn, :] * jnp.exp(laters[n])
+        kk = k_ref[rn, :].astype(jnp.float32)
+        weighted = kk * rest
+        for h in range(heads):
+            lk, lv = slice(h * width, (h + 1) * width), slice(h * span, (h + 1) * span)
+            dks[rn, lk] += rest[:, lk] * product(v_ref[rn, lv], following[h], 1, 0)
+            dv[rn, lv] = (dvs[rn, lv] + product(weighted[:, lk], following[h], 1, 1)).astype(jnp.bfloat16)
+        full_k = dks[rn, :]
+        dk[rn, :] = full_k.astype(jnp.bfloat16)
+        dqs[rn, :] = q_ref[rn, :].astype(jnp.float32) * scale * dqs[rn, :] - kk * full_k
+    sums = [jnp.sum(dqs[n * SPAN : (n + 1) * SPAN, :], axis=0, keepdims=True) for n in range(blocks)]
+    total = sums[0]
+    for n in range(1, blocks):
+        total = total + sums[n]
+    sum_out[...] = jnp.broadcast_to(total, sum_out.shape)
+    for j in range(3):
+        start(s > j, sum_out, sum_in.at[s], u_send.at[j], u_recv.at[s], at(j, me))
+    ones_up = upper.astype(jnp.float32)
+    behind = jnp.zeros_like(total)
+    for n in reversed(range(blocks)):
+        rn = slice(n * SPAN, (n + 1) * SPAN)
+        dks[rn, :] = exact(ones_up, dqs[rn, :]) + behind
+        behind = behind + sums[n]
+    ends[0:1, :] = jnp.zeros_like(total)
+    for source in (3, 2, 1):
+
+        @pl.when(s < source)
+        def _():
+            arrived(sum_in.at[source], u_recv.at[source])
+            ends[0:1, :] += sum_in[source, 0:1, :]
+
+    da[...] = dks[...] + ends[0:1, :]
+    for when, parts in sent:
+        if when is None:
+            copy(*parts).wait_send()
+        else:
+
+            @pl.when(when)
+            def _():
+                copy(*parts).wait_send()
+
+
+def tail(token_grad, out_proj, mixer_output, queries, key_rows, value_rows, log_decay, entry):
+    tokens, columns = token_grad.shape
+    heads, width, span = entry.shape
+    keys = heads * width
+    n_sp = lax.axis_size("sp")
+    depth = out_proj.shape[0] // n_sp
+    blocks = tokens // SPAN
+    bf16, f32 = jnp.bfloat16, jnp.float32
+    dma = pltpu.SemaphoreType.DMA
+    vmem = pl.BlockSpec(memory_space=pltpu.VMEM)
+    return pl.pallas_call(
+        tail_kernel,
+        out_shape=(
+            jax.ShapeDtypeStruct((depth, columns), f32),
+            jax.ShapeDtypeStruct((tokens, keys), bf16),
+            jax.ShapeDtypeStruct((tokens, keys), bf16),
+            jax.ShapeDtypeStruct((tokens, columns), bf16),
+            jax.ShapeDtypeStruct((tokens, keys), f32),
+        ),
+        in_specs=[vmem] * 8,
+        out_specs=(vmem,) * 5,
+        scratch_shapes=[
+            pltpu.VMEM((8, tokens, columns), bf16),
+            pltpu.VMEM((2, n_sp * tokens, columns), bf16),
+            pltpu.VMEM((n_sp * tokens, columns), bf16),
+            pltpu.VMEM((tokens, columns), f32),
+            pltpu.VMEM((tokens, columns), bf16),
+            *[pltpu.VMEM((tokens, keys), f32) for _ in range(6)],
+            pltpu.VMEM((heads, tokens, SPAN), f32),
+            pltpu.VMEM((heads, blocks, span, width), f32),
+            pltpu.VMEM((8, keys), f32),
+            pltpu.VMEM((tokens, keys), f32),
+            pltpu.VMEM((tokens, keys), f32),
+            pltpu.VMEM((tokens, columns), f32),
+            pltpu.VMEM((heads, span, width), bf16),
+            pltpu.VMEM((n_sp, heads, span, width), bf16),
+            pltpu.VMEM((heads, span, width), f32),
+            pltpu.VMEM((8, keys), f32),
+            pltpu.VMEM((n_sp, 8, keys), f32),
+            pltpu.VMEM((8, keys), f32),
+            pltpu.VMEM((n_sp, 8, keys), f32),
+            dma((2, 3)),
+            dma((2, 3)),
+            dma((4,)),
+            dma((4,)),
+            dma((4,)),
+            dma((4,)),
+            dma((3,)),
+            dma((3,)),
+            dma((3,)),
+            dma((3,)),
+            dma((2, 3)),
+            dma((2, 4)),
+            dma((3,)),
+            dma((4,)),
+            dma((3,)),
+            dma((4,)),
+        ],
+        compiler_params=pltpu.CompilerParams(
+            collective_id=2, has_side_effects=True, vmem_limit_bytes=60 * 1024 * 1024
+        ),
+        name="tail",
+    )(token_grad, out_proj, mixer_output, queries, key_rows, value_rows, log_decay, entry)
+
+
 def dense_experts(layer_input, out_cotangent, routes, route_weights, gate_proj, up_proj, down_proj, log_decay):
     n_sp, tp = lax.axis_size("sp"), lax.axis_size("tp")
     nz = tp // 2
@@ -767,11 +1156,24 @@
 ):
     args = (layer_input, out_cotangent, routes, route_weights, gate_proj, up_proj, down_proj)
     paired = lax.axis_size("sp") == 4 and lax.axis_size("tp") % 2 == 0
-    if paired and gate_proj.shape[0] == 1 and log_decay.shape[1] == routes.shape[0]:
+    square = paired and lax.axis_size("tp") == 8 and gate_proj.shape[0] == 1
+    square = square and log_decay.shape[1] == routes.shape[0]
+    if square:
         parts, token_grad, kept = dense_experts(*args, log_decay)
-        kept = kept.reshape(kept.shape[0], *entry_state.shape[1:3])
     else:
         parts, token_grad, kept = routed_experts(*args)
+    if square:
+        outs = tail(
+            token_grad,
+            out_proj,
+            mixer_output,
+            queries,
+            key_rows,
+            value_rows,
+            log_decay,
+            entry_state[0],
+        )
+        return (*parts, *outs)
     full_grad = lax.all_gather(token_grad, "tp", axis=1, tiled=True)
     partial = jnp.einsum(
         "td,tc->dc", full_grad, mixer_output, preferred_element_type=jnp.float32

time: 295 us -> 233 us (0.79)
  Pallas kernels: 173 us -> 222 us
  matrix products: 31.5 us -> 0 us
  blocking collectives: 23.8 us -> 0 us
  waiting for transfers between devices: 22.9 us -> 0 us
  between operations: 14.5 us -> 0.7 us
  other arithmetic: 12.1 us -> 1.72 us
  local copies, waits for them, and re-layouts: 14.3 us -> 8.32 us
    pallas_call x0 -> x1, Pallas kernels: none -> 48.7 us  [tail(): pl.pallas_call(tail_kernel, out_shape=(jax.ShapeDtypeStruct((depth, colum...]
    dot_general x41 -> x0, matrix products: 31.5 us -> none  [the longest x4 6.84 us: reverse_block(): jnp.einsum('hts,thk->shk', dots_now, query_raised, precision=PRECISION_LE...]
    all_gather x2 -> x0, blocking collectives: 23.8 us -> none  [the longest x1 15.9 us: entering(): gathered = (kept, lax.all_gather(value[1].astype(jnp.bfloat16), axis))]
    reduce_scatter x1 -> x0, waiting for transfers between devices: 12.9 us -> none  [body(): lax.psum_scatter(partial, 'sp', scatter_dimension=0, tiled=True)]
    all_gather x1 -> x0, waiting for transfers between devices: 9.97 us -> none  [body(): full_grad = lax.all_gather(token_grad, 'tp', axis=1, tiled=True)]
    another operation x15 -> x0, other arithmetic: 6.6 us -> none  [the longest x4 3.68 us: reverse_block(): running_decay = jnp.cumsum(decay_now, axis=0)]
  transfers between devices with their start and end apart: 2 -> 0, of which waited for: 2 -> 0; matrix products, arithmetic and copies ran while one was open for 7% -> 0% of each run, Pallas kernels for 5% -> 0%
where the time goes in v1:
time: 233 us
  Pallas kernels  222 us (95%)
  local copies, waits for them, and re-layouts  8.32 us (4%)
    pallas_call x1, Pallas kernels, gather_all(): pl.pallas_call(functools.partial(gather_kernel, nz), out_shape=(tokens, t...  90.7 us
    pallas_call x1, Pallas kernels, reduce_all(): pl.pallas_call(functools.partial(reduce_kernel, nz), out_shape=jax.ShapeD...  53.5 us
    pallas_call x1, Pallas kernels, tail(): pl.pallas_call(tail_kernel, out_shape=(jax.ShapeDtypeStruct((depth, colum...  48.7 us
    pallas_call x1, Pallas kernels, hidden_deltas(): pl.pallas_call(hidden_kernel, grid=(tp,), out_shape=(tall, tall, wide, wi...  15.3 us
    pallas_call x1, Pallas kernels, weight_grads(): pl.pallas_call(weight_kernel, grid=(tp,), out_shape=(tall, tall, wide), i...  13.5 us
    unnamed x13, local copies, waits for them, and re-layouts  5.88 us

profile of v1, /device:TPU:0, one launch (start us, length us, event | category | flops | bytes accessed | tf_op | source)
XLA Modules:
  0.0 232.5 jit_solution(18354488496131247244)
XLA Ops:
  0.6 1.0 reduce_sum.49
  1.6 0.7 fusion.3
  2.4 0.6 pad.4.w_ref
  3.0 90.7 %gather_all.1 = (bf16[4,8,256,512]{3,2,1,0:T(8,128)(2,1)}, bf16[4,8,256,512]{3,2,1,0:T(8,128)(2,1)}, f32[4,8,256]{2,1,0:T(8,128)}, bf16[4,512,256]{2,1,0:T(8,128)(2,1)}, bf16[4,512,256]{2,1,0:T(8,128)(2,1)}) custom-call(bf16[256,512]{1,0:T(8,128)(2,1)} %x_ref.1, bf16[256,512]{1,0:T(8,128)(2,1)} %g_ref.3, f32[8,256]{1,0:T(8,128)} %pad.4.w_ref, ...), custom_call_target="tpu_custom_call" | custom-call | tf_op jit(solution)/shard_map/gather_all/pallas_call | solution.py:397
  93.7 0.8 constant_dynamic-slice_fusion
  94.5 1.0 copy.23.w_ref
  95.5 15.3 %hidden_deltas.1 = (bf16[1024,256]{1,0:T(8,128)(2,1)}, bf16[1024,256]{1,0:T(8,128)(2,1)}, bf16[256,1024]{1,0:T(8,128)(2,1)}, bf16[256,1024]{1,0:T(8,128)(2,1)}, bf16[256,1024]{1,0:T(8,128)(2,1)}) custom-call(bf16[4,8,256,512]{3,2,1,0:T(8,128)(2,1)} %get-tuple-element.26.x_ref, bf16[4,8,256,512]{3,2,1,0:T(8,128)(2,1)} %get-tuple-element.27.g_ref, ...), custom_call_target="tpu_custom_call" | custom-call | flops 6442450944 | bytes 16777216 | tf_op jit(solution)/shard_map/hidden_deltas/pallas_call | solution.py:479
  110.8 53.5 %reduce_all.1.tg = bf16[256,512]{1,0:T(8,128)(2,1)} custom-call(bf16[1024,256]{1,0:T(8,128)(2,1)} %get-tuple-element.35.gd, bf16[1024,256]{1,0:T(8,128)(2,1)} %get-tuple-element.36.ud, bf16[4,2,512,256]{3,2,1,0:T(8,128)(2,1)} %bitcast.17, bf16[4,2,512,256]{3,2,1,0:T(8,128)(2,1)} %bitcast.20, bf16[4,512,256]{2,1,0:T(8,128)(2,1)} %get-tuple-element.37.wgp, ...), custom_call_target="tpu_custom_call" | custom-call | tf_op jit(solution)/shard_map/reduce_all/pallas_call | solution.py:656
  164.3 13.5 %weight_grads.1 = (bf16[4096,256]{1,0:T(8,128)(2,1)}, bf16[4096,256]{1,0:T(8,128)(2,1)}, bf16[256,4096]{1,0:T(8,128)(2,1)}) custom-call(bf16[4,8,256,512]{3,2,1,0:T(8,128)(2,1)} %get-tuple-element.26.x_ref, bf16[4,8,256,512]{3,2,1,0:T(8,128)(2,1)} %get-tuple-element.27.g_ref, f32[1024,1]{1,0:T(8,128)} %copy.23.w_ref, ...), custom_call_target="tpu_custom_call" | custom-call | flops 6442450944 | bytes 16777216 | tf_op jit(solution)/shard_map/weight_grads/pallas_call | solution.py:509
  177.8 48.7 %tail.1 = (f32[1024,512]{1,0:T(8,128)}, bf16[256,256]{1,0:T(8,128)(2,1)}, bf16[256,256]{1,0:T(8,128)(2,1)}, bf16[256,512]{1,0:T(8,128)(2,1)}, f32[256,256]{1,0:T(8,128)}) custom-call(bf16[256,512]{1,0:T(8,128)(2,1)} %reduce_all.1.tg, bf16[4096,512]{1,0:T(8,128)(2,1)} %wo.1, bf16[256,512]{1,0:T(8,128)(2,1)} %mo.1, bf16[256,256]{1,0:T(8,128)(2,1)} %q_ref.1, ...), custom_call_target="tpu_custom_call" | custom-call | tf_op jit(solution)/shard_map/tail/pallas_call | solution.py:1018
  226.6 0.0 copy-start.3
  226.6 0.0 copy-start.2
  226.6 0.0 copy-start.1
  226.6 0.0 copy-start
  226.6 3.1 %copy.29 = f32[1024,512]{1,0:T(8,128)} copy(f32[1024,512]{1,0:T(8,128)} %get-tuple-element.59) | data formatting | bytes 4194304
  229.8 0.0 copy-done.3
  229.8 0.7 copy.30
  230.4 0.0 copy-done.2
  230.4 0.7 copy.31
  231.1 0.0 copy-done.1
  231.1 0.7 copy.32
  231.8 0.0 copy-done
  231.8 0.7 copy.33
  (2 shorter events, 0.0 us)
Async XLA Ops:
  226.6 3.2 %copy-start.3 = (bf16[256,256]{1,0:T(8,128)(2,1)S(1)}, bf16[256,256]{1,0:T(8,128)(2,1)}, u32[]{:S(2)}) copy-start(bf16[256,256]{1,0:T(8,128)(2,1)} %get-tuple-element.60) | copy-start | bytes 393220
  226.6 3.8 %copy-start.2 = (bf16[256,256]{1,0:T(8,128)(2,1)S(1)}, bf16[256,256]{1,0:T(8,128)(2,1)}, u32[]{:S(2)}) copy-start(bf16[256,256]{1,0:T(8,128)(2,1)} %get-tuple-element.61) | copy-start | bytes 393220
  226.6 4.5 %copy-start.1 = (bf16[256,512]{1,0:T(8,128)(2,1)S(1)}, bf16[256,512]{1,0:T(8,128)(2,1)}, u32[]{:S(2)}) copy-start(bf16[256,512]{1,0:T(8,128)(2,1)} %get-tuple-element.62) | copy-start | bytes 786436
  226.6 5.2 %copy-start = (f32[256,256]{1,0:T(8,128)S(1)}, f32[256,256]{1,0:T(8,128)}, u32[]{:S(2)}) copy-start(f32[256,256]{1,0:T(8,128)} %get-tuple-element.63) | copy-start | bytes 786436

commit v2 on v1

--- a/solution.py
+++ b/solution.py
@@ -243,442 +243,14 @@
     return {"sp": s, "tp": t}
 
 
-def gather_kernel(
-    nz,
-    x_ref,
-    g_ref,
-    w_ref,
-    wg_ref,
-    wu_ref,
-    xo,
-    go,
-    wo,
-    wgo,
-    wuo,
-    z_send,
-    z_recv,
-    p_send,
-    p_recv,
-    d_send,
-    d_recv,
-    w_send,
-    w_recv,
-    t_send,
-    t_recv,
-    own_sem,
-):
-    s, sy, sx, sd, z, c = peers(nz)
-    me, partner = z * 2 + c, z * 2 + 1 - c
-    greet(
-        [at(s, lax.rem(z + d, nz) * 2 + c) for d in range(1, nz)]
-        + [at(sy, me), at(sx, me), at(sd, me), at(s, partner)]
-    )
-    sources, outs = (x_ref, g_ref), (xo, go)
-    first, second = (sy, sx), (sx, sy)
-    sent = []
-
-    def copy(src, dst, send, recv, device):
-        return pltpu.make_async_remote_copy(
-            src_ref=src, dst_ref=dst, send_sem=send, recv_sem=recv, device_id=device, device_id_type=MESH
-        )
-
-    def start(*parts):
-        made = copy(*parts)
-        made.start()
-        sent.append(made)
-
-    def column(k):
-        return lax.rem(z + k, nz) * 2 + c
-
-    def source(a, k):
-        return sources[a] if k == 0 else outs[a].at[s, column(k)]
-
-    def plane(a, k, j, src, row, target):
-        start(
-            src,
-            outs[a].at[row, column(k)],
-            p_send.at[a, k, j],
-            p_recv.at[a, k, j],
-            at(target, me),
-        )
-
-    def arrived(a, k, j, row):
-        slot = outs[a].at[row, column(k)]
-        copy(slot, slot, p_send.at[a, k, j], p_recv.at[a, k, j], at(s, partner)).wait_recv()
-        return slot
-
-    def across(a, k, j, src, row):
-        start(
-            src,
-            outs[a].at[row, column(k)],
-            d_send.at[a, k, j],
-            d_recv.at[a, k, j],
-            at(s, partner),
-        )
-
-    def open_step(k):
-        if k:
-            for a in range(2):
-                slot = outs[a].at[s, column(k)]
-                copy(slot, slot, z_send.at[a, k - 1], z_recv.at[a, k - 1], at(s, partner)).wait_recv()
-        for a in range(2):
-            plane(a, k, 0, source(a, k), s, first[a])
-        for a in range(2):
-            plane(a, k, 1, source(a, k), s, second[a])
-        for a in range(2):
-            across(a, k, 0, source(a, k), s)
-
-    def middle_step(k):
-        for a in range(2):
-            slot = arrived(a, k, 0, first[a])
-            plane(a, k, 2, slot, first[a], second[a])
-            across(a, k, 1, slot, first[a])
-
-    def close_step(k):
-        for a in range(2):
-            across(a, k, 2, arrived(a, k, 1, second[a]), second[a])
-        for a in range(2):
-            across(a, k, 3, arrived(a, k, 2, sd), sd)
-
-    for j, target in enumerate((sy, sx, sd)):
-        start(w_ref, wo.at[s], w_send.at[j], w_recv.at[j], at(target, me))
-    open_step(0)
-    for d in range(1, nz):
-        for a in range(2):
-            start(
-                sources[a],
-                outs[a].at[s, me],
-                z_send.at[a, d - 1],
-                z_recv.at[a, d - 1],
-                at(s, lax.rem(z + nz - d, nz) * 2 + c),
-            )
-    local = [
-        pltpu.make_async_copy(x_ref, xo.at[s, me], own_sem.at[0]),
-        pltpu.make_async_copy(g_ref, go.at[s, me], own_sem.at[1]),
-        pltpu.make_async_copy(w_ref, wo.at[s], own_sem.at[2]),
-    ]
-    for one in local:
-        one.start()
-    for k in range(nz):
-        for i, (src, dst) in enumerate(((wg_ref, wgo), (wu_ref, wuo))):
-            start(src.at[k, 1 - c], dst.at[k], t_send.at[i, k], t_recv.at[i, k], at(s, partner))
-    middle_step(0)
-    for k in range(1, nz):
-        open_step(k)
-        close_step(k - 1)
-        middle_step(k)
-    close_step(nz - 1)
-    for j, row in enumerate((sy, sx, sd)):
-        slot = wo.at[row]
-        copy(slot, slot, w_send.at[j], w_recv.at[j], at(s, partner)).wait_recv()
-    for k in range(nz):
-        for i, dst in enumerate((wgo, wuo)):
-            slot = dst.at[k]
-            copy(slot, slot, t_send.at[i, k], t_recv.at[i, k], at(s, partner)).wait_recv()
-        for a in range(2):
-            for j, row in enumerate((s, first[a], second[a], sd)):
-                slot = outs[a].at[row, lax.rem(z + k, nz) * 2 + 1 - c]
-                copy(slot, slot, d_send.at[a, k, j], d_recv.at[a, k, j], at(s, partner)).wait_recv()
-    for one in sent:
-        one.wait_send()
-    for one in local:
-        one.wait()
-
-
-def gather_all(layer_input, out_cotangent, table, gate_rows, up_rows):
-    nz = gate_rows.shape[0]
-    rows, columns = layer_input.shape
-    n_sp = lax.axis_size("sp")
-    dma = pltpu.SemaphoreType.DMA
-    vmem = pl.BlockSpec(memory_space=pltpu.VMEM)
-    anywhere = pl.BlockSpec(memory_space=pl.ANY)
-    tokens = jax.ShapeDtypeStruct((n_sp, 2 * nz, rows, columns), layer_input.dtype)
-    halves = jax.ShapeDtypeStruct((nz,) + gate_rows.shape[2:], gate_rows.dtype)
-    return pl.pallas_call(
-        functools.partial(gather_kernel, nz),
-        out_shape=(
-            tokens,
-            tokens,
-            jax.ShapeDtypeStruct((n_sp,) + table.shape, table.dtype),
-            halves,
-            halves,
-        ),
-        in_specs=[vmem, vmem, vmem, anywhere, anywhere],
-        out_specs=(anywhere,) * 5,
-        scratch_shapes=[
-            dma((2, nz - 1)),
-            dma((2, nz - 1)),
-            dma((2, nz, 3)),
-            dma((2, nz, 3)),
-            dma((2, nz, 4)),
-            dma((2, nz, 4)),
-            dma((3,)),
-            dma((3,)),
-            dma((2, nz)),
-            dma((2, nz)),
-            dma((3,)),
-        ],
-        compiler_params=pltpu.CompilerParams(collective_id=0, has_side_effects=True),
-        name="gather_all",
-    )(layer_input, out_cotangent, table, gate_rows, up_rows)
-
-
 def dots(left, right, left_dim, right_dim):
     return lax.dot_general(
         left, right, (((left_dim,), (right_dim,)), ((), ())), preferred_element_type=jnp.float32
     )
 
 
-def hidden_kernel(
-    x_ref, g_ref, w_ref, wg_ref, wu_ref, wd_ref, gd, ud, gdt, udt, ht, gate, up, back
-):
-    step = pl.program_id(0)
-    rows = gate.shape[0]
-    columns = x_ref.shape[-1]
-
-    @pl.when(step == 0)
-    def _():
-        for total in (gate, up, back):
-            total[...] = jnp.zeros_like(total)
-
-    x = x_ref[...].reshape(rows, columns)
-    pair = (w_ref[...] * g_ref[...].reshape(rows, columns).astype(jnp.float32)).astype(jnp.bfloat16)
-    gate[...] += dots(x, wg_ref[...], 1, 0)
-    up[...] += dots(x, wu_ref[...], 1, 0)
-    back[...] += dots(pair, wd_ref[...], 1, 1)
-
-    @pl.when(step == pl.num_programs(0) - 1)
-    def _():
-        gate_pre, up_pre, grad = gate[...], up[...], back[...]
-        sigmoid_gate = jax.nn.sigmoid(gate_pre)
-        activated = gate_pre * sigmoid_gate
-        gate_delta = grad * up_pre * sigmoid_gate * (1.0 + gate_pre * (1.0 - sigmoid_gate))
-        up_delta = grad * activated
-        gd[...] = gate_delta.astype(jnp.bfloat16)
-        ud[...] = up_delta.astype(jnp.bfloat16)
-        gdt[...] = gate_delta.T.astype(jnp.bfloat16)
-        udt[...] = up_delta.T.astype(jnp.bfloat16)
-        ht[...] = (activated * up_pre).T.astype(jnp.bfloat16)
-
-
-def token_spec(tokens):
-    return pl.BlockSpec((tokens.shape[0], 1) + tokens.shape[2:], lambda t: (0, t, 0, 0))
-
-
 def fixed_spec(shape):
     return pl.BlockSpec(shape, lambda t: (0,) * len(shape))
-
-
-def hidden_deltas(x, g, weight, gate_w, up_w, down_w):
-    n_sp, tp, rows, columns = x.shape
-    total, hidden = n_sp * rows, gate_w.shape[1]
-    tall = jax.ShapeDtypeStruct((total, hidden), jnp.bfloat16)
-    wide = jax.ShapeDtypeStruct((hidden, total), jnp.bfloat16)
-    down_spec = pl.BlockSpec((hidden, columns), lambda t: (0, t))
-    row_spec = pl.BlockSpec((columns, hidden), lambda t: (t, 0))
-    return pl.pallas_call(
-        hidden_kernel,
-        grid=(tp,),
-        out_shape=(tall, tall, wide, wide, wide),
-        in_specs=[token_spec(x), token_spec(g), fixed_spec((total, 1)), row_spec, row_spec, down_spec],
-        out_specs=[fixed_spec(tall.shape)] * 2 + [fixed_spec(wide.shape)] * 3,
-        scratch_shapes=[pltpu.VMEM((total, hidden), jnp.float32)] * 3,
-        cost_estimate=pl.CostEstimate(
-            flops=6 * total * hidden * tp * columns, bytes_accessed=4 * x.size, transcendentals=0
-        ),
-        name="hidden_deltas",
-    )(x, g, weight, gate_w, up_w, down_w)
-
-
-def weight_kernel(x_ref, g_ref, w_ref, gdt, udt, ht, gate_out, up_out, down_out):
-    rows = w_ref.shape[0]
-    columns = x_ref.shape[-1]
-    x = x_ref[...].reshape(rows, columns)
-    pair = (w_ref[...] * g_ref[...].reshape(rows, columns).astype(jnp.float32)).astype(jnp.bfloat16)
-    gate_out[...] = dots(gdt[...], x, 1, 0).T.astype(jnp.bfloat16)
-    up_out[...] = dots(udt[...], x, 1, 0).T.astype(jnp.bfloat16)
-    down_out[...] = dots(ht[...], pair, 1, 0).astype(jnp.bfloat16)
-
-
-def weight_grads(x, g, weight, gdt, udt, ht):
-    n_sp, tp, rows, columns = x.shape
-    total, hidden = n_sp * rows, gdt.shape[0]
-    tall = jax.ShapeDtypeStruct((tp * columns, hidden), jnp.bfloat16)
-    wide = jax.ShapeDtypeStruct((hidden, tp * columns), jnp.bfloat16)
-    row_spec = pl.BlockSpec((columns, hidden), lambda t: (t, 0))
-    return pl.pallas_call(
-        weight_kernel,
-        grid=(tp,),
-        out_shape=(tall, tall, wide),
-        in_specs=[token_spec(x), token_spec(g), fixed_spec((total, 1))] + [fixed_spec(gdt.shape)] * 3,
-        out_specs=[row_spec, row_spec, pl.BlockSpec((hidden, columns), lambda t: (0, t))],
-        cost_estimate=pl.CostEstimate(
-            flops=6 * total * hidden * tp * columns, bytes_accessed=4 * x.size, transcendentals=0
-        ),
-        name="weight_grads",
-    )(x, g, weight, gdt, udt, ht)
-
-
-def reduce_kernel(
-    nz,
-    gd,
-    ud,
-    wg,
-    wu,
-    wgp,
-    wup,
-    g_ref,
-    out,
-    other,
-    s1,
-    r1,
-    keep,
-    s2,
-    r2,
-    zs,
-    zr,
-    o_send,
-    o_recv,
-    a_send,
-    a_recv,
-    b_send,
-    b_recv,
-    z_send,
-    z_recv,
-):
-    s, sy, sx, sd, z, c = peers(nz)
-    me, partner = z * 2 + c, z * 2 + 1 - c
-    rows = g_ref.shape[0]
-    half = rows // 2
-    greet(
-        [at(s, lax.rem(z + d, nz) * 2 + c) for d in range(1, nz)]
-        + [at(sy, me), at(sx, me), at(s, partner)]
-    )
-    sent = []
-
-    def start(src, dst, send, recv, device):
-        made = pltpu.make_async_remote_copy(
-            src_ref=src, dst_ref=dst, send_sem=send, recv_sem=recv, device_id=device, device_id_type=MESH
-        )
-        made.start()
-        sent.append(made)
-        return made
-
-    swaps = [
-        start(ref, other.at[i], o_send.at[i], o_recv.at[i], at(s, partner))
-        for i, ref in enumerate((gd, ud))
-    ]
-    for one in swaps:
-        one.wait_recv()
-    first, second = (sy, sx), (sx, sy)
-    outgoing, crossing, final = {}, {}, {}
-
-    def compute(k):
-        column = lax.rem(z + nz - k, nz)
-        weights = (wg[column, c], wu[column, c], wgp[column], wup[column])
-        for i, q in enumerate((s, sy, sx, sd)):
-            span = pl.ds(pl.multiple_of(q * rows, rows), rows)
-            lefts = (gd[span, :], ud[span, :], other[0, span, :], other[1, span, :])
-            tile = dots(lefts[0], weights[0], 1, 1)
-            for left, weight in zip(lefts[1:], weights[1:]):
-                tile = tile + dots(left, weight, 1, 1)
-            for a in range(2):
-                part = tile[a * half : (a + 1) * half]
-                if i == 0:
-                    keep[k, a, 0] = part
-                elif i == 3:
-                    s1[k, a, 1] = part.astype(jnp.bfloat16)
-                elif i == 1 + a:
-                    s1[k, a, 0] = part.astype(jnp.bfloat16)
-                else:
-                    keep[k, a, 1] = part
-        for a in range(2):
-            outgoing[k, a] = start(
-                s1.at[k, a], r1.at[k, a], a_send.at[k, a], a_recv.at[k, a], at(first[a], me)
-            )
-
-    def middle(k):
-        for a in range(2):
-            outgoing[k, a].wait_recv()
-            s2[k, a] = (keep[k, a, 1] + r1[k, a, 1].astype(jnp.float32)).astype(jnp.bfloat16)
-            crossing[k, a] = start(
-                s2.at[k, a], r2.at[k, a], b_send.at[k, a], b_recv.at[k, a], at(second[a], me)
-            )
-
-    def close(k):
-        for a in range(2):
-            crossing[k, a].wait_recv()
-            total = (
-                keep[k, a, 0]
-                + r1[k, a, 0].astype(jnp.float32)
-                + r2[k, a].astype(jnp.float32)
-            )
-            if k:
-                zs[k - 1, a * half : (a + 1) * half] = total.astype(jnp.bfloat16)
-            else:
-                keep[k, a, 0] = total
-        if k:
-            final[k] = start(
-                zs.at[k - 1],
-                zr.at[k - 1],
-                z_send.at[k - 1],
-                z_recv.at[k - 1],
-                at(s, lax.rem(z + nz - k, nz) * 2 + c),
-            )
-
-    order = list(range(1, nz)) + [0]
-    for i in range(nz + 2):
-        if i < nz:
-            compute(order[i])
-        if 0 <= i - 2 < nz:
-            close(order[i - 2])
-        if 0 <= i - 1 < nz:
-            middle(order[i - 1])
-    for k in range(1, nz):
-        final[k].wait_recv()
-    for a in range(2):
-        span = slice(a * half, (a + 1) * half)
-        total = keep[0, a, 0]
-        for k in range(1, nz):
-            total = total + zr[k - 1, span].astype(jnp.float32)
-        out[span] = (g_ref[span].astype(jnp.float32) + total).astype(jnp.bfloat16)
-    for one in sent:
-        one.wait_send()
-
-
-def reduce_all(gd, ud, gate_rows, up_rows, gate_other, up_other, out_cotangent):
-    nz = gate_rows.shape[0]
-    rows, columns = out_cotangent.shape
-    half = rows // 2
-    dma = pltpu.SemaphoreType.DMA
-    vmem = pl.BlockSpec(memory_space=pltpu.VMEM)
-    bf16 = jnp.bfloat16
-    return pl.pallas_call(
-        functools.partial(reduce_kernel, nz),
-        out_shape=jax.ShapeDtypeStruct((rows, columns), bf16),
-        in_specs=[vmem] * 7,
-        out_specs=vmem,
-        scratch_shapes=[
-            pltpu.VMEM((2,) + gd.shape, bf16),
-            pltpu.VMEM((nz, 2, 2, half, columns), bf16),
-            pltpu.VMEM((nz, 2, 2, half, columns), bf16),
-            pltpu.VMEM((nz, 2, 2, half, columns), jnp.float32),
-            pltpu.VMEM((nz, 2, half, columns), bf16),
-            pltpu.VMEM((nz, 2, half, columns), bf16),
-            pltpu.VMEM((nz - 1, rows, columns), bf16),
-            pltpu.VMEM((nz - 1, rows, columns), bf16),
-            dma((2,)),
-            dma((2,)),
-            dma((nz, 2)),
-            dma((nz, 2)),
-            dma((nz, 2)),
-            dma((nz, 2)),
-            dma((nz - 1,)),
-            dma((nz - 1,)),
-        ],
-        compiler_params=pltpu.CompilerParams(collective_id=1, has_side_effects=True),
-        name="reduce_all",
-    )(gd, ud, gate_rows, up_rows, gate_other, up_other, out_cotangent)
 
 
 def pieces(value):
@@ -1070,25 +642,418 @@
     )(token_grad, out_proj, mixer_output, queries, key_rows, value_rows, log_decay, entry)
 
 
-def dense_experts(layer_input, out_cotangent, routes, route_weights, gate_proj, up_proj, down_proj, log_decay):
-    n_sp, tp = lax.axis_size("sp"), lax.axis_size("tp")
-    nz = tp // 2
-    columns = layer_input.shape[1]
-    hidden = gate_proj.shape[2]
-    rows = [
-        jnp.sum(jnp.where(routes == e, route_weights, 0.0), axis=1) for e in range(n_sp)
-    ] + [jnp.exp(jnp.sum(log_decay, axis=0))]
-    table = jnp.pad(jnp.stack(rows), ((0, -len(rows) % 8), (0, 0)))
-    gate_rows = gate_proj.reshape(nz, 2, columns, hidden)
-    up_rows = up_proj.reshape(nz, 2, columns, hidden)
-    x, g, tables, gate_other, up_other = gather_all(
-        layer_input, out_cotangent, table, gate_rows, up_rows
-    )
-    weight = lax.dynamic_index_in_dim(tables, lax.axis_index("sp"), 1, False).reshape(-1, 1)
-    gd, ud, gdt, udt, ht = hidden_deltas(x, g, weight, gate_proj[0], up_proj[0], down_proj[0])
-    token_grad = reduce_all(gd, ud, gate_rows, up_rows, gate_other, up_other, out_cotangent)
-    grads = weight_grads(x, g, weight, gdt, udt, ht)
-    return [part[None] for part in grads], token_grad, tables[:, n_sp]
+def front_kernel(
+    cap,
+    x_ref,
+    g_ref,
+    routes,
+    weights,
+    wg_hbm,
+    wu_hbm,
+    wd_hbm,
+    out,
+    x_out,
+    g_out,
+    gdt,
+    udt,
+    ht,
+    wg,
+    wu,
+    wd,
+    wgp,
+    wup,
+    tok,
+    snd,
+    xr,
+    gr,
+    pick,
+    back_pick,
+    share,
+    gate,
+    up,
+    back,
+    delta,
+    other,
+    tiles,
+    landed,
+    keep,
+    zs,
+    zr,
+    w_sem,
+    h_sem,
+    z_send,
+    z_recv,
+    p_send,
+    p_recv,
+    o_send,
+    o_recv,
+    t_send,
+    t_recv,
+    d_send,
+    d_recv,
+    a_send,
+    a_recv,
+    b_send,
+    b_recv,
+):
+    nz = 4
+    s, sy, sx, sd, z, c = peers(nz)
+    me, partner = z * 2 + c, z * 2 + 1 - c
+    tokens, columns = x_ref.shape
+    greet(
+        [at(s, lax.rem(z + d, nz) * 2 + c) for d in range(1, nz)]
+        + [at(sy, me), at(sx, me), at(sd, me), at(s, partner)]
+    )
+    sent, local = [], []
+    around = (sd, sy, sx)
+    rows_of = (xr, gr)
+
+    def copy(src, dst, send, recv, device):
+        return pltpu.make_async_remote_copy(
+            src_ref=src, dst_ref=dst, send_sem=send, recv_sem=recv, device_id=device, device_id_type=MESH
+        )
+
+    def start(when, *parts):
+        def go():
+            copy(*parts).start()
+
+        if when is None:
+            go()
+        else:
+            pl.when(when)(go)
+        sent.append((when, parts))
+
+    def arrived(slot, recv):
+        copy(slot, slot, recv, recv, at(s, partner)).wait_recv()
+
+    def slots(index):
+        return pl.ds(pl.multiple_of(index * cap, 32), cap)
+
+    def lines(index):
+        return pl.ds(pl.multiple_of(index * columns, columns), columns)
+
+    turns = [(z, 0 * z)]
+    turns.append((jnp.where(z == 0, 1, z - 1), jnp.where(z == 0, 1, 0)))
+    turns.append(
+        (
+            jnp.where(z == 0, 2, jnp.where(z == nz - 1, z - 2, z + 1)),
+            jnp.where(z == nz - 1, 0, 1),
+        )
+    )
+    turns.append((jnp.where(z < 2, 3, 0), jnp.where(z < 2, 1, 0)))
+
+    def hop(when, src, a, block, way):
+        target = z + 1 - 2 * way
+        room = (target >= 0) & (target < nz)
+        start(
+            room if when is None else when & room,
+            src,
+            tok.at[a, block],
+            z_send.at[a, way, block],
+            z_recv.at[a, block],
+            at(s, target * 2 + c),
+        )
+
+    for way in range(2):
+        hop(None, x_ref, 0, z, way)
+        hop(None, g_ref, 1, z, way)
+    loads = [
+        pltpu.make_async_copy(src.at[0], dst, w_sem.at[i])
+        for i, (src, dst) in enumerate(((wg_hbm, wg), (wu_hbm, wu), (wd_hbm, wd)))
+    ]
+    for one in loads:
+        one.start()
+
+    expert = lax.broadcasted_iota(jnp.int32, (8, tokens), 0)
+    first, second = routes[0:1, :] == expert, routes[1:2, :] == expert
+    named = jnp.where(first | second, 1.0, 0.0)
+    worth = jnp.where(first, weights[0:1, :], 0.0) + jnp.where(second, weights[1:2, :], 0.0)
+    earlier = lax.broadcasted_iota(jnp.int32, (tokens, tokens), 0) < lax.broadcasted_iota(
+        jnp.int32, (tokens, tokens), 1
+    )
+    rank = dots(
+        named.astype(jnp.bfloat16), jnp.where(earlier, 1.0, 0.0).astype(jnp.bfloat16), 1, 0
+    )
+    rank = jnp.where(named > 0.5, rank, -1.0)
+    place = lax.broadcasted_iota(jnp.int32, (cap, tokens), 0).astype(jnp.float32)
+    for e in range(4):
+        hit = rank[e : e + 1, :] == place
+        chosen = jnp.where(hit, 1.0, 0.0)
+        pick[e * cap : (e + 1) * cap, :] = chosen.astype(jnp.bfloat16)
+        back_pick[e] = chosen.T.astype(jnp.bfloat16)
+        share[e * cap : (e + 1) * cap, :] = jnp.broadcast_to(
+            jnp.sum(jnp.where(hit, worth[e : e + 1, :], 0.0), axis=1, keepdims=True), (cap, 128)
+        )
+
+    def pieces_of(src, a, e):
+        rows = dots(pick[slots(e), :], src, 1, 0)
+        if a:
+            rows = rows * share[slots(e), 0:1]
+        return rows.astype(jnp.bfloat16)
+
+    def dispatch(i):
+        block, way = turns[i]
+        mine = block * 2 + c
+        for a in range(2):
+            if i:
+                arrived(tok.at[a, block], z_recv.at[a, block])
+                hop(None, tok.at[a, block], a, block, way)
+        for a in range(2):
+            src = (x_ref, g_ref)[a][...] if i == 0 else tok[a, block]
+            for j, e in enumerate(around):
+                snd[i, a, j] = pieces_of(src, a, e)
+                start(
+                    None,
+                    snd.at[i, a, j],
+                    rows_of[a].at[mine, slots(s)],
+                    p_send.at[i, a, j],
+                    p_recv.at[i, a, j],
+                    at(e, me),
+                )
+            rows_of[a][mine, slots(s), :] = pieces_of(src, a, s)
+            hand(i, a, 3, s)
+
+    def hand(i, a, j, row):
+        spot = rows_of[a].at[turns[i][0] * 2 + c, slots(row)]
+        start(None, spot, spot, o_send.at[i, a, j], o_recv.at[i, a, j], at(s, partner))
+
+    def receive(i):
+        for a in range(2):
+            for j, e in enumerate(around):
+                arrived(rows_of[a].at[turns[i][0] * 2 + c, slots(e)], p_recv.at[i, a, j])
+                hand(i, a, j, e)
+
+    def compute(i, side):
+        block = turns[i][0] * 2 + (1 - c if side else c)
+        if side:
+            for a in range(2):
+                for j, e in enumerate(around + (s,)):
+                    arrived(rows_of[a].at[block, slots(e)], o_recv.at[i, a, j])
+        sums = (
+            dots(xr[block], wg[lines(block), :], 1, 0),
+            dots(xr[block], wu[lines(block), :], 1, 0),
+            dots(gr[block], wd[:, lines(block)], 1, 1),
+        )
+        for total, part in zip((gate, up, back), sums):
+            if i == 0 and side == 0:
+                total[...] = part
+            else:
+                total[...] += part
+        for a, (src, dst) in enumerate(((xr, x_out), (gr, g_out))):
+            made = pltpu.make_async_copy(src.at[block], dst.at[block], h_sem.at[i, side, a])
+            made.start()
+            local.append(made)
+
+    dispatch(0)
+    for one in loads:
+        one.wait()
+    for k in range(nz):
+        for i, (src, dst) in enumerate(((wg, wgp), (wu, wup))):
+            start(
+                None, src.at[lines(k * 2 + 1 - c)], dst.at[k], t_send.at[i, k], t_recv.at[i, k], at(s, partner)
+            )
+    for i in range(1, nz):
+        dispatch(i)
+        receive(i - 1)
+        compute(i - 1, 0)
+        compute(i - 1, 1)
+    receive(nz - 1)
+    compute(nz - 1, 0)
+    compute(nz - 1, 1)
+
+    gate_pre, up_pre, grad = gate[...], up[...], back[...]
+    sigmoid_gate = jax.nn.sigmoid(gate_pre)
+    activated = gate_pre * sigmoid_gate
+    gate_delta = grad * up_pre * sigmoid_gate * (1.0 + gate_pre * (1.0 - sigmoid_gate))
+    up_delta = grad * activated
+    delta[0] = gate_delta.astype(jnp.bfloat16)
+    delta[1] = up_delta.astype(jnp.bfloat16)
+    gate[...] = gate_delta
+    up[...] = up_delta
+    back[...] = activated * up_pre
+    for i in range(2):
+        start(None, delta.at[i], other.at[i], d_send.at[i], d_recv.at[i], at(s, partner))
+    gdt[...] = gate[...].T.astype(jnp.bfloat16)
+    udt[...] = up[...].T.astype(jnp.bfloat16)
+    ht[...] = back[...].T.astype(jnp.bfloat16)
+    for k in range(nz):
+        for i, dst in enumerate((wgp, wup)):
+            arrived(dst.at[k], t_recv.at[i, k])
+    for i in range(2):
+        arrived(other.at[i], d_recv.at[i])
+
+    order = list(range(1, nz)) + [0]
+
+    def target(k):
+        return lax.rem(z + k, nz)
+
+    def produce(i):
+        column = target(order[i])
+        here = lines(column * 2 + c)
+        pairs = (
+            (delta.at[0], wg[here, :]),
+            (delta.at[1], wu[here, :]),
+            (other.at[0], wgp[column]),
+            (other.at[1], wup[column]),
+        )
+        for j, e in enumerate(around + (s,)):
+            tile = None
+            for left, right in pairs:
+                part = dots(left[slots(e), :], right, 1, 1)
+                tile = part if tile is None else tile + part
+            if j < 3:
+                tiles[i, j] = tile.astype(jnp.bfloat16)
+                start(
+                    None,
+                    tiles.at[i, j],
+                    landed.at[i, slots(s)],
+                    a_send.at[i, j],
+                    a_recv.at[i, j],
+                    at(e, me),
+                )
+            else:
+                landed[i, slots(s), :] = tile.astype(jnp.bfloat16)
+
+    def collect(i):
+        k = order[i]
+        for j, e in enumerate(around):
+            arrived(landed.at[i, slots(e)], a_recv.at[i, j])
+        total = None
+        for e in range(4):
+            part = dots(back_pick[e], landed[i, e * cap : (e + 1) * cap, :], 1, 0)
+            total = part if total is None else total + part
+        if k:
+            zs[k - 1] = total.astype(jnp.bfloat16)
+            start(
+                None,
+                zs.at[k - 1],
+                zr.at[k - 1],
+                b_send.at[k - 1],
+                b_recv.at[k - 1],
+                at(s, target(k) * 2 + c),
+            )
+        else:
+            keep[...] = total
+
+    produce(0)
+    for i in range(1, nz):
+        produce(i)
+        collect(i - 1)
+    collect(nz - 1)
+    total = g_ref[...].astype(jnp.float32) + keep[...]
+    for k in range(1, nz):
+        arrived(zr.at[k - 1], b_recv.at[k - 1])
+        total = total + zr[k - 1].astype(jnp.float32)
+    out[...] = total.astype(jnp.bfloat16)
+    for one in local:
+        one.wait()
+    for when, parts in sent:
+        if when is None:
+            copy(*parts).wait_send()
+        else:
+
+            @pl.when(when)
+            def _():
+                copy(*parts).wait_send()
+
+
+def front(layer_input, out_cotangent, routes, route_weights, gate_proj, up_proj, down_proj):
+    tokens, columns = layer_input.shape
+    width, hidden = gate_proj.shape[1:]
+    tp = width // columns
+    cap = 5 * routes.shape[1] * tokens // (4 * lax.axis_size("sp"))
+    total = 4 * cap
+    bf16, f32 = jnp.bfloat16, jnp.float32
+    dma = pltpu.SemaphoreType.DMA
+    vmem = pl.BlockSpec(memory_space=pltpu.VMEM)
+    anywhere = pl.BlockSpec(memory_space=pl.ANY)
+    rows = jax.ShapeDtypeStruct((tp, total, columns), bf16)
+    wide = jax.ShapeDtypeStruct((hidden, total), bf16)
+    return pl.pallas_call(
+        functools.partial(front_kernel, cap),
+        out_shape=(jax.ShapeDtypeStruct((tokens, columns), bf16), rows, rows, wide, wide, wide),
+        in_specs=[vmem] * 4 + [anywhere] * 3,
+        out_specs=(vmem, anywhere, anywhere, vmem, vmem, vmem),
+        scratch_shapes=[
+            pltpu.VMEM((width, hidden), bf16),
+            pltpu.VMEM((width, hidden), bf16),
+            pltpu.VMEM((hidden, width), bf16),
+            pltpu.VMEM((4, columns, hidden), bf16),
+            pltpu.VMEM((4, columns, hidden), bf16),
+            pltpu.VMEM((2, 4, tokens, columns), bf16),
+            pltpu.VMEM((4, 2, 3, cap, columns), bf16),
+            pltpu.VMEM((tp, total, columns), bf16),
+            pltpu.VMEM((tp, total, columns), bf16),
+            pltpu.VMEM((total, tokens), bf16),
+            pltpu.VMEM((4, tokens, cap), bf16),
+            pltpu.VMEM((total, 128), f32),
+            pltpu.VMEM((total, hidden), f32),
+            pltpu.VMEM((total, hidden), f32),
+            pltpu.VMEM((total, hidden), f32),
+            pltpu.VMEM((2, total, hidden), bf16),
+            pltpu.VMEM((2, total, hidden), bf16),
+            pltpu.VMEM((4, 3, cap, columns), bf16),
+            pltpu.VMEM((4, total, columns), bf16),
+            pltpu.VMEM((tokens, columns), f32),
+            pltpu.VMEM((3, tokens, columns), bf16),
+            pltpu.VMEM((3, tokens, columns), bf16),
+            dma((3,)),
+            dma((4, 2, 2)),
+            dma((2, 2, 4)),
+            dma((2, 4)),
+            dma((4, 2, 3)),
+            dma((4, 2, 3)),
+            dma((4, 2, 4)),
+            dma((4, 2, 4)),
+            dma((2, 4)),
+            dma((2, 4)),
+            dma((2,)),
+            dma((2,)),
+            dma((4, 3)),
+            dma((4, 3)),
+            dma((3,)),
+            dma((3,)),
+        ],
+        compiler_params=pltpu.CompilerParams(
+            collective_id=0, has_side_effects=True, vmem_limit_bytes=60 * 1024 * 1024
+        ),
+        name="front",
+    )(layer_input, out_cotangent, routes.T, route_weights.T, gate_proj, up_proj, down_proj)
+
+
+def weight_kernel(x_ref, g_ref, gdt, udt, ht, gate_out, up_out, down_out):
+    x, pair = x_ref[0], g_ref[0]
+    gate_out[...] = dots(gdt[...], x, 1, 0).T.astype(jnp.bfloat16)
+    up_out[...] = dots(udt[...], x, 1, 0).T.astype(jnp.bfloat16)
+    down_out[...] = dots(ht[...], pair, 1, 0).astype(jnp.bfloat16)
+
+
+def weight_grads(x, g, gdt, udt, ht):
+    tp, rows, columns = x.shape
+    hidden = gdt.shape[0]
+    tall = jax.ShapeDtypeStruct((tp * columns, hidden), jnp.bfloat16)
+    wide = jax.ShapeDtypeStruct((hidden, tp * columns), jnp.bfloat16)
+    row_spec = pl.BlockSpec((columns, hidden), lambda t: (t, 0))
+    token = pl.BlockSpec((1, rows, columns), lambda t: (t, 0, 0))
+    return pl.pallas_call(
+        weight_kernel,
+        grid=(tp,),
+        out_shape=(tall, tall, wide),
+        in_specs=[token, token] + [fixed_spec(gdt.shape)] * 3,
+        out_specs=[row_spec, row_spec, pl.BlockSpec((hidden, columns), lambda t: (0, t))],
+        cost_estimate=pl.CostEstimate(
+            flops=6 * rows * hidden * tp * columns, bytes_accessed=4 * x.size, transcendentals=0
+        ),
+        name="weight_grads",
+    )(x, g, gdt, udt, ht)
+
+
+def dense_experts(layer_input, out_cotangent, routes, route_weights, gate_proj, up_proj, down_proj):
+    token_grad, x, g, gdt, udt, ht = front(
+        layer_input, out_cotangent, routes, route_weights, gate_proj, up_proj, down_proj
+    )
+    grads = weight_grads(x, g, gdt, udt, ht)
+    return [part[None] for part in grads], token_grad, None
 
 
 def routed_experts(
@@ -1159,7 +1124,7 @@
     square = paired and lax.axis_size("tp") == 8 and gate_proj.shape[0] == 1
     square = square and log_decay.shape[1] == routes.shape[0]
     if square:
-        parts, token_grad, kept = dense_experts(*args, log_decay)
+        parts, token_grad, kept = dense_experts(*args)
     else:
         parts, token_grad, kept = routed_experts(*args)
     if square:

time: 233 us -> 180 us (0.77)
  Pallas kernels: 222 us -> 173 us
  local copies, waits for them, and re-layouts: 8.32 us -> 5.88 us
    pallas_call x3 -> x1, Pallas kernels: 159 us -> 109 us  [front(): pl.pallas_call(functools.partial(front_kernel, cap), out_shape=(jax.Shape...]
    pallas_call x1, Pallas kernels: 48.7 us -> 53.4 us  [tail(): pl.pallas_call(tail_kernel, out_shape=(jax.ShapeDtypeStruct((depth, colum...]
    pallas_call x1, Pallas kernels: 13.5 us -> 10.7 us  [weight_grads(): pl.pallas_call(weight_kernel, grid=(tp,), out_shape=(tall, tall, wide), i...]
where the time goes in v2:
time: 180 us; the launch traced here: 179 us
  Pallas kernels  173 us (96%)
  local copies, waits for them, and re-layouts  5.88 us (3%)
    pallas_call x1, Pallas kernels, front(): pl.pallas_call(functools.partial(front_kernel, cap), out_shape=(jax.Shape...  109 us
    pallas_call x1, Pallas kernels, tail(): pl.pallas_call(tail_kernel, out_shape=(jax.ShapeDtypeStruct((depth, colum...  53.4 us
    pallas_call x1, Pallas kernels, weight_grads(): pl.pallas_call(weight_kernel, grid=(tp,), out_shape=(tall, tall, wide), i...  10.7 us
    unnamed x13, local copies, waits for them, and re-layouts  5.88 us

profile of v2, /device:TPU:0, one launch (start us, length us, event | category | flops | bytes accessed | tf_op | source)
XLA Modules:
  0.0 179.3 jit_solution(13605394135129172030)
XLA Ops:
  0.6 108.7 %front.1 = (bf16[256,512]{1,0:T(8,128)(2,1)}, bf16[8,640,512]{2,1,0:T(8,128)(2,1)}, bf16[8,640,512]{2,1,0:T(8,128)(2,1)}, bf16[256,640]{1,0:T(8,128)(2,1)}, bf16...) custom-call(bf16[256,512]{1,0:T(8,128)(2,1)} %x_ref.1, bf16[256,512]{1,0:T(8,128)(2,1)} %g_ref.1, s32[2,256]{1,0:T(2,128)} %bitcast.7, ...), custom_call_target="tpu_custom_call" | custom-call | tf_op jit(solution)/shard_map/front/pallas_call | solution.py:972
  109.3 10.7 %weight_grads.1 = (bf16[4096,256]{1,0:T(8,128)(2,1)}, bf16[4096,256]{1,0:T(8,128)(2,1)}, bf16[256,4096]{1,0:T(8,128)(2,1)}) custom-call(bf16[8,640,512]{2,1,0:T(8,128)(2,1)} %get-tuple-element.22.x_ref, bf16[8,640,512]{2,1,0:T(8,128)(2,1)} %get-tuple-element.23.g_ref, bf16[256,640]{1,0:T(8,128)(2,1)} %get-tuple-element.24.gdt, ...), custom_call_target="tpu_custom_call" | custom-call | flops 4026531840 | bytes 10485760 | tf_op jit(solution)/shard_map/weight_grads/pallas_call | solution.py:1038
  120.0 53.4 %tail.1 = (f32[1024,512]{1,0:T(8,128)}, bf16[256,256]{1,0:T(8,128)(2,1)}, bf16[256,256]{1,0:T(8,128)(2,1)}, bf16[256,512]{1,0:T(8,128)(2,1)}, f32[256,256]{1,0:T(8,128)}) custom-call(bf16[256,512]{1,0:T(8,128)(2,1)} %get-tuple-element.30.tg, bf16[4096,512]{1,0:T(8,128)(2,1)} %wo.1, bf16[256,512]{1,0:T(8,128)(2,1)} %mo.1, bf16[256,256]{1,0:T(8,128)(2,1)} %q_ref.1, ...), custom_call_target="tpu_custom_call" | custom-call | tf_op jit(solution)/shard_map/tail/pallas_call | solution.py:590
  173.4 0.0 copy-start.3
  173.4 0.0 copy-start.2
  173.4 0.0 copy-start.1
  173.5 0.0 copy-start
  173.5 3.1 %copy.27 = f32[1024,512]{1,0:T(8,128)} copy(f32[1024,512]{1,0:T(8,128)} %get-tuple-element.47) | data formatting | bytes 4194304
  176.6 0.0 copy-done.3
  176.6 0.7 copy.28
  177.3 0.0 copy-done.2
  177.3 0.7 copy.29
  177.9 0.0 copy-done.1
  177.9 0.7 copy.30
  178.6 0.0 copy-done
  178.6 0.7 copy.31
Async XLA Ops:
  173.4 3.2 %copy-start.3 = (bf16[256,256]{1,0:T(8,128)(2,1)S(1)}, bf16[256,256]{1,0:T(8,128)(2,1)}, u32[]{:S(2)}) copy-start(bf16[256,256]{1,0:T(8,128)(2,1)} %get-tuple-element.48) | copy-start | bytes 393220
  173.4 3.8 %copy-start.2 = (bf16[256,256]{1,0:T(8,128)(2,1)S(1)}, bf16[256,256]{1,0:T(8,128)(2,1)}, u32[]{:S(2)}) copy-start(bf16[256,256]{1,0:T(8,128)(2,1)} %get-tuple-element.49) | copy-start | bytes 393220
  173.4 4.5 %copy-start.1 = (bf16[256,512]{1,0:T(8,128)(2,1)S(1)}, bf16[256,512]{1,0:T(8,128)(2,1)}, u32[]{:S(2)}) copy-start(bf16[256,512]{1,0:T(8,128)(2,1)} %get-tuple-element.50) | copy-start | bytes 786436
  173.5 5.2 %copy-start = (f32[256,256]{1,0:T(8,128)S(1)}, f32[256,256]{1,0:T(8,128)}, u32[]{:S(2)}) copy-start(f32[256,256]{1,0:T(8,128)} %get-tuple-element.51) | copy-start | bytes 786436

commit v3 on v2

--- a/solution.py
+++ b/solution.py
@@ -247,10 +247,6 @@
     return lax.dot_general(
         left, right, (((left_dim,), (right_dim,)), ((), ())), preferred_element_type=jnp.float32
     )
-
-
-def fixed_spec(shape):
-    return pl.BlockSpec(shape, lambda t: (0,) * len(shape))
 
 
 def pieces(value):
@@ -372,39 +368,53 @@
     def arrived(slot, recv):
         copy(slot, slot, recv, recv, at(s, partner)).wait_recv()
 
-    def slot(block, core):
-        return full.at[block * 2 + core]
+    half = tokens // 2
+
+    def slot(block, core, part):
+        return full.at[block * 2 + core, part * half : (part + 1) * half]
 
     def rows(index):
         return pl.ds(pl.multiple_of(index * tokens, tokens), tokens)
 
-    def spread(when, src, block):
-        start(when, src, slot(block, c), b_send.at[block], b_recv.at[block], at(s, partner))
+    def half_rows(index, part):
+        return pl.ds(pl.multiple_of(index * tokens + part * half, half), half)
+
+    def spread(when, src, block, part):
+        start(
+            when,
+            src,
+            slot(block, c, part),
+            b_send.at[block, part],
+            b_recv.at[block, part],
+            at(s, partner),
+        )
         ok = block != s
         start(
             ok if when is None else when & ok,
             src,
-            tgd.at[c, rows(s)],
-            p_send.at[block],
-            p_recv.at[s],
+            tgd.at[c, half_rows(s, part)],
+            p_send.at[block, part],
+            p_recv.at[s, part],
             at(block, me),
         )
 
-    def hop(when, src, block, way, d):
+    def hop(when, src, block, way, d, part):
         step = 1 if way == 0 else -1
         room = z + step < nz if way == 0 else z + step >= 0
         start(
             room if when is None else when & room,
             src,
-            slot(block, c),
-            z_send.at[way, d],
-            z_recv.at[way, d],
+            slot(block, c, part),
+            z_send.at[way, d, part],
+            z_recv.at[way, d, part],
             at(s, (z + step) * 2 + c),
         )
 
-    hop(None, tg, z, 0, 0)
-    hop(None, tg, z, 1, 0)
-    spread(None, tg, z)
+    for part in range(2):
+        own = tg.at[part * half : (part + 1) * half]
+        hop(None, own, z, 0, 0, part)
+        hop(None, own, z, 1, 0, part)
+        spread(None, own, z, part)
     for j, target in enumerate((sy, sx, sd)):
         start(None, mo, moa.at[rows(s)], m_send.at[j], m_recv.at[j], at(target, me))
 
@@ -459,27 +469,34 @@
         else:
             mg[...] += part
 
+    def crossed(block):
+        for part in range(2):
+            arrived(slot(block, 1 - c, part), b_recv.at[block, part])
+
     mix(z, c, True)
     full[me] = tg[...]
-    arrived(slot(z, 1 - c), b_recv.at[z])
+    crossed(z)
     mix(z, 1 - c)
     for d in range(1, nz):
         for way in range(2):
             block = z - d if way == 0 else z + d
             here = block >= 0 if way == 0 else block < nz
 
-            @pl.when(here)
-            def _():
-                arrived(slot(block, c), z_recv.at[way, d - 1])
-
-            if d < nz - 1:
-                hop(here, slot(block, c), block, way, d)
-            spread(here, slot(block, c), block)
+            for part in range(2):
+                spot = slot(block, c, part)
+
+                @pl.when(here)
+                def _():
+                    arrived(spot, z_recv.at[way, d - 1, part])
+
+                if d < nz - 1:
+                    hop(here, spot, block, way, d, part)
+                spread(here, spot, block, part)
 
             @pl.when(here)
             def _():
                 mix(block, c)
-                arrived(slot(block, 1 - c), b_recv.at[block])
+                crossed(block)
                 mix(block, 1 - c)
 
     gb[...] = mg[...].astype(jnp.bfloat16)
@@ -510,7 +527,8 @@
 
     for j, other in enumerate((sy, sx, sd)):
         block = tgd.at[c, rows(other)]
-        arrived(block, p_recv.at[other])
+        for part in range(2):
+            arrived(tgd.at[c, half_rows(other, part)], p_recv.at[other, part])
         start(None, block, block, t_send.at[j], t_recv.at[j], at(s, partner))
         arrived(moa.at[rows(other)], m_recv.at[j])
     moa[rows(s), :] = mo[...]
@@ -618,12 +636,12 @@
             pltpu.VMEM((n_sp, 8, keys), f32),
             pltpu.VMEM((8, keys), f32),
             pltpu.VMEM((n_sp, 8, keys), f32),
-            dma((2, 3)),
-            dma((2, 3)),
-            dma((4,)),
-            dma((4,)),
-            dma((4,)),
-            dma((4,)),
+            dma((2, 3, 2)),
+            dma((2, 3, 2)),
+            dma((4, 2)),
+            dma((4, 2)),
+            dma((4, 2)),
+            dma((4, 2)),
             dma((3,)),
             dma((3,)),
             dma((3,)),
@@ -636,7 +654,7 @@
             dma((4,)),
         ],
         compiler_params=pltpu.CompilerParams(
-            collective_id=2, has_side_effects=True, vmem_limit_bytes=60 * 1024 * 1024
+            collective_id=2, has_side_effects=True, vmem_limit_bytes=24 * 1024 * 1024
         ),
         name="tail",
     )(token_grad, out_proj, mixer_output, queries, key_rows, value_rows, log_decay, entry)
@@ -652,11 +670,15 @@
     wu_hbm,
     wd_hbm,
     out,
-    x_out,
-    g_out,
+    gate_out,
+    up_out,
+    down_out,
     gdt,
     udt,
     ht,
+    gate_grad,
+    up_grad,
+    down_grad,
     wg,
     wu,
     wd,
@@ -683,6 +705,8 @@
     h_sem,
     z_send,
     z_recv,
+    y_send,
+    y_recv,
     p_send,
     p_recv,
     o_send,
@@ -704,7 +728,7 @@
         [at(s, lax.rem(z + d, nz) * 2 + c) for d in range(1, nz)]
         + [at(sy, me), at(sx, me), at(sd, me), at(s, partner)]
     )
-    sent, local = [], []
+    sent = []
     around = (sd, sy, sx)
     rows_of = (xr, gr)
 
@@ -742,21 +766,28 @@
     )
     turns.append((jnp.where(z < 2, 3, 0), jnp.where(z < 2, 1, 0)))
 
-    def hop(when, src, a, block, way):
+    middle = (z > 0) & (z < nz - 1)
+
+    def room(way):
         target = z + 1 - 2 * way
-        room = (target >= 0) & (target < nz)
-        start(
-            room if when is None else when & room,
+        return (target >= 0) & (target < nz)
+
+    def hop(src, a, block, way):
+        return (
             src,
             tok.at[a, block],
             z_send.at[a, way, block],
             z_recv.at[a, block],
-            at(s, target * 2 + c),
-        )
+            at(s, (z + 1 - 2 * way) * 2 + c),
+        )
+
+    def relay_hop(block, way):
+        spot = gr.at[block * 2 + c, slots(sd)]
+        return (spot, spot, y_send.at[way, block], y_recv.at[block], at(s, (z + 1 - 2 * way) * 2 + c))
 
     for way in range(2):
-        hop(None, x_ref, 0, z, way)
-        hop(None, g_ref, 1, z, way)
+        start(room(way), *hop(x_ref, 0, z, way))
+        start(room(way), *hop(g_ref, 1, z, way))
     loads = [
         pltpu.make_async_copy(src.at[0], dst, w_sem.at[i])
         for i, (src, dst) in enumerate(((wg_hbm, wg), (wu_hbm, wu), (wd_hbm, wd)))
@@ -791,60 +822,106 @@
             rows = rows * share[slots(e), 0:1]
         return rows.astype(jnp.bfloat16)
 
-    def dispatch(i):
+    def guarded(when, go):
+        if when is None:
+            go()
+        else:
+            pl.when(when)(go)
+
+    def take(when, i, a):
         block, way = turns[i]
-        mine = block * 2 + c
-        for a in range(2):
-            if i:
-                arrived(tok.at[a, block], z_recv.at[a, block])
-                hop(None, tok.at[a, block], a, block, way)
-        for a in range(2):
-            src = (x_ref, g_ref)[a][...] if i == 0 else tok[a, block]
-            for j, e in enumerate(around):
-                snd[i, a, j] = pieces_of(src, a, e)
-                start(
-                    None,
-                    snd.at[i, a, j],
-                    rows_of[a].at[mine, slots(s)],
-                    p_send.at[i, a, j],
-                    p_recv.at[i, a, j],
-                    at(e, me),
-                )
-            rows_of[a][mine, slots(s), :] = pieces_of(src, a, s)
-            hand(i, a, 3, s)
+        parts = hop(tok.at[a, block], a, block, way)
+
+        def go():
+            arrived(tok.at[a, block], z_recv.at[a, block])
+            pl.when(room(way))(lambda: copy(*parts).start())
+
+        guarded(when, go)
+
+    def relay(when, i):
+        block, way = turns[i]
+        spot = gr.at[block * 2 + c, slots(sd)]
+
+        def go():
+            if i == 0:
+                arrived(spot, p_recv.at[0, 1, 0])
+                for both in range(2):
+                    parts = relay_hop(block, both)
+                    pl.when(room(both))(lambda parts=parts: copy(*parts).start())
+            else:
+                arrived(spot, y_recv.at[block])
+                parts = relay_hop(block, way)
+                pl.when(room(way))(lambda: copy(*parts).start())
+            copy(*handed(i, 1, 0, sd)).start()
+
+        guarded(when, go)
+
+    def dispatch(i, a):
+        mine = turns[i][0] * 2 + c
+        src = (x_ref, g_ref)[a][...] if i == 0 else tok[a, turns[i][0]]
+        for j, e in enumerate(around):
+            if i and a and j == 0:
+                continue
+            snd[i, a, j] = pieces_of(src, a, e)
+            start(
+                None,
+                snd.at[i, a, j],
+                rows_of[a].at[mine, slots(s)],
+                p_send.at[i, a, j],
+                p_recv.at[i, a, j],
+                at(e, me),
+            )
+        rows_of[a][mine, slots(s), :] = pieces_of(src, a, s)
+        hand(i, a, 3, s)
+
+    def handed(i, a, j, row):
+        spot = rows_of[a].at[turns[i][0] * 2 + c, slots(row)]
+        return (spot, spot, o_send.at[i, a, j], o_recv.at[i, a, j], at(s, partner))
 
     def hand(i, a, j, row):
-        spot = rows_of[a].at[turns[i][0] * 2 + c, slots(row)]
-        start(None, spot, spot, o_send.at[i, a, j], o_recv.at[i, a, j], at(s, partner))
-
-    def receive(i):
-        for a in range(2):
-            for j, e in enumerate(around):
-                arrived(rows_of[a].at[turns[i][0] * 2 + c, slots(e)], p_recv.at[i, a, j])
-                hand(i, a, j, e)
-
-    def compute(i, side):
+        start(None, *handed(i, a, j, row))
+
+    for i in range(nz):
+        block, way = turns[i]
+        if i:
+            for a in range(2):
+                sent.append((room(way), hop(tok.at[a, block], a, block, way)))
+        for one in range(2) if i == 0 else (way,):
+            sent.append((room(one), relay_hop(block, one)))
+        sent.append((None, handed(i, 1, 0, sd)))
+
+    def receive(i, a):
+        for j, e in enumerate(around):
+            if a and j == 0:
+                continue
+            arrived(rows_of[a].at[turns[i][0] * 2 + c, slots(e)], p_recv.at[i, a, j])
+            hand(i, a, j, e)
+
+    def compute(i, side, a):
         block = turns[i][0] * 2 + (1 - c if side else c)
         if side:
-            for a in range(2):
-                for j, e in enumerate(around + (s,)):
-                    arrived(rows_of[a].at[block, slots(e)], o_recv.at[i, a, j])
-        sums = (
-            dots(xr[block], wg[lines(block), :], 1, 0),
-            dots(xr[block], wu[lines(block), :], 1, 0),
-            dots(gr[block], wd[:, lines(block)], 1, 1),
-        )
-        for total, part in zip((gate, up, back), sums):
+            for j, e in enumerate(around + (s,)):
+                arrived(rows_of[a].at[block, slots(e)], o_recv.at[i, a, j])
+        if a:
+            sums = ((back, dots(gr[block], wd[:, lines(block)], 1, 1)),)
+        else:
+            sums = tuple(
+                (total, dots(xr[block], w[lines(block), :], 1, 0)) for total, w in ((gate, wg), (up, wu))
+            )
+        for total, part in sums:
             if i == 0 and side == 0:
                 total[...] = part
             else:
                 total[...] += part
-        for a, (src, dst) in enumerate(((xr, x_out), (gr, g_out))):
-            made = pltpu.make_async_copy(src.at[block], dst.at[block], h_sem.at[i, side, a])
-            made.start()
-            local.append(made)
-
-    dispatch(0)
+
+    def finish_block(i):
+        for a in range(2):
+            receive(i, a)
+            compute(i, 0, a)
+            compute(i, 1, a)
+
+    dispatch(0, 0)
+    dispatch(0, 1)
     for one in loads:
         one.wait()
     for k in range(nz):
@@ -852,14 +929,29 @@
             start(
                 None, src.at[lines(k * 2 + 1 - c)], dst.at[k], t_send.at[i, k], t_recv.at[i, k], at(s, partner)
             )
-    for i in range(1, nz):
-        dispatch(i)
-        receive(i - 1)
-        compute(i - 1, 0)
-        compute(i - 1, 1)
-    receive(nz - 1)
-    compute(nz - 1, 0)
-    compute(nz - 1, 1)
+    ends = jnp.logical_not(middle)
+    for a in range(2):
+        take(None, 1, a)
+        dispatch(1, a)
+    for a in range(2):
+        take(middle, 2, a)
+    relay(None, 0)
+    finish_block(0)
+    for a in range(2):
+        take(ends, 2, a)
+        dispatch(2, a)
+    for a in range(2):
+        take(middle, 3, a)
+    relay(None, 1)
+    finish_block(1)
+    for a in range(2):
+        take(ends, 3, a)
+        dispatch(3, a)
+    relay(None, 2)
+    relay(middle, 3)
+    finish_block(2)
+    relay(ends, 3)
+    finish_block(3)
 
     gate_pre, up_pre, grad = gate[...], up[...], back[...]
     sigmoid_gate = jax.nn.sigmoid(gate_pre)
@@ -935,18 +1027,35 @@
         else:
             keep[...] = total
 
-    produce(0)
-    for i in range(1, nz):
+    def saves(block):
+        return (
+            (gate_grad.at[lines(block), :], gate_out.at[lines(block), :], h_sem.at[0, block]),
+            (up_grad.at[lines(block), :], up_out.at[lines(block), :], h_sem.at[1, block]),
+            (down_grad.at[block], down_out.at[:, lines(block)], h_sem.at[2, block]),
+        )
+
+    def weigh(block, _):
+        x, pair = xr[block], gr[block]
+        gate_grad[lines(block), :] = dots(gdt[...], x, 1, 0).T.astype(jnp.bfloat16)
+        up_grad[lines(block), :] = dots(udt[...], x, 1, 0).T.astype(jnp.bfloat16)
+        down_grad[block] = dots(ht[...], pair, 1, 0).astype(jnp.bfloat16)
+        for one in saves(block):
+            pltpu.make_async_copy(*one).start()
+        return 0
+
+    for i in range(nz):
         produce(i)
-        collect(i - 1)
-    collect(nz - 1)
+    for i in range(nz):
+        lax.fori_loop(2 * i, 2 * i + 2, weigh, 0)
+        collect(i)
     total = g_ref[...].astype(jnp.float32) + keep[...]
     for k in range(1, nz):
         arrived(zr.at[k - 1], b_recv.at[k - 1])
         total = total + zr[k - 1].astype(jnp.float32)
     out[...] = total.astype(jnp.bfloat16)
-    for one in local:
-        one.wait()
+    for block in range(2 * nz):
+        for one in saves(block):
+            pltpu.make_async_copy(*one).wait()
     for when, parts in sent:
         if when is None:
             copy(*parts).wait_send()
@@ -967,14 +1076,23 @@
     dma = pltpu.SemaphoreType.DMA
     vmem = pl.BlockSpec(memory_space=pltpu.VMEM)
     anywhere = pl.BlockSpec(memory_space=pl.ANY)
-    rows = jax.ShapeDtypeStruct((tp, total, columns), bf16)
-    wide = jax.ShapeDtypeStruct((hidden, total), bf16)
     return pl.pallas_call(
         functools.partial(front_kernel, cap),
-        out_shape=(jax.ShapeDtypeStruct((tokens, columns), bf16), rows, rows, wide, wide, wide),
+        out_shape=(
+            jax.ShapeDtypeStruct((tokens, columns), bf16),
+            jax.ShapeDtypeStruct((width, hidden), bf16),
+            jax.ShapeDtypeStruct((width, hidden), bf16),
+            jax.ShapeDtypeStruct((hidden, width), bf16),
+        ),
         in_specs=[vmem] * 4 + [anywhere] * 3,
-        out_specs=(vmem, anywhere, anywhere, vmem, vmem, vmem),
+        out_specs=(vmem, anywhere, anywhere, anywhere),
         scratch_shapes=[
+            pltpu.VMEM((hidden, total), bf16),
+            pltpu.VMEM((hidden, total), bf16),
+            pltpu.VMEM((hidden, total), bf16),
+            pltpu.VMEM((width, hidden), bf16),
+            pltpu.VMEM((width, hidden), bf16),
+            pltpu.VMEM((tp, hidden, columns), bf16),
             pltpu.VMEM((width, hidden), bf16),
             pltpu.VMEM((width, hidden), bf16),
             pltpu.VMEM((hidden, width), bf16),
@@ -998,9 +1116,11 @@
             pltpu.VMEM((3, tokens, columns), bf16),
             pltpu.VMEM((3, tokens, columns), bf16),
             dma((3,)),
-            dma((4, 2, 2)),
+            dma((3, 8)),
             dma((2, 2, 4)),
             dma((2, 4)),
+            dma((2, 4)),
+            dma((4,)),
             dma((4, 2, 3)),
             dma((4, 2, 3)),
             dma((4, 2, 4)),
@@ -1015,45 +1135,36 @@
             dma((3,)),
         ],
         compiler_params=pltpu.CompilerParams(
-            collective_id=0, has_side_effects=True, vmem_limit_bytes=60 * 1024 * 1024
+            collective_id=0, has_side_effects=True, vmem_limit_bytes=52 * 1024 * 1024
         ),
         name="front",
     )(layer_input, out_cotangent, routes.T, route_weights.T, gate_proj, up_proj, down_proj)
 
 
-def weight_kernel(x_ref, g_ref, gdt, udt, ht, gate_out, up_out, down_out):
-    x, pair = x_ref[0], g_ref[0]
-    gate_out[...] = dots(gdt[...], x, 1, 0).T.astype(jnp.bfloat16)
-    up_out[...] = dots(udt[...], x, 1, 0).T.astype(jnp.bfloat16)
-    down_out[...] = dots(ht[...], pair, 1, 0).astype(jnp.bfloat16)
-
-
-def weight_grads(x, g, gdt, udt, ht):
-    tp, rows, columns = x.shape
-    hidden = gdt.shape[0]
-    tall = jax.ShapeDtypeStruct((tp * columns, hidden), jnp.bfloat16)
-    wide = jax.ShapeDtypeStruct((hidden, tp * columns), jnp.bfloat16)
-    row_spec = pl.BlockSpec((columns, hidden), lambda t: (t, 0))
-    token = pl.BlockSpec((1, rows, columns), lambda t: (t, 0, 0))
+def finish_kernel(*refs):
+    count = len(refs) // 2
+    sems = refs[-1]
+    moves = [
+        pltpu.make_async_copy(src, dst, sems.at[n])
+        for n, (src, dst) in enumerate(zip(refs[:count], refs[count : 2 * count]))
+    ]
+    for one in moves:
+        one.start()
+    for one in moves:
+        one.wait()
+
+
+def finish(*arrays):
+    anywhere = pl.BlockSpec(memory_space=pl.ANY)
     return pl.pallas_call(
-        weight_kernel,
-        grid=(tp,),
-        out_shape=(tall, tall, wide),
-        in_specs=[token, token] + [fixed_spec(gdt.shape)] * 3,
-        out_specs=[row_spec, row_spec, pl.BlockSpec((hidden, columns), lambda t: (0, t))],
-        cost_estimate=pl.CostEstimate(
-            flops=6 * rows * hidden * tp * columns, bytes_accessed=4 * x.size, transcendentals=0
-        ),
-        name="weight_grads",
-    )(x, g, gdt, udt, ht)
-
-
-def dense_experts(layer_input, out_cotangent, routes, route_weights, gate_proj, up_proj, down_proj):
-    token_grad, x, g, gdt, udt, ht = front(
-        layer_input, out_cotangent, routes, route_weights, gate_proj, up_proj, down_proj
-    )
-    grads = weight_grads(x, g, gdt, udt, ht)
-    return [part[None] for part in grads], token_grad, None
+        finish_kernel,
+        out_shape=tuple(jax.ShapeDtypeStruct(one.shape, one.dtype) for one in arrays),
+        in_specs=[pl.BlockSpec(memory_space=pltpu.VMEM)] * len(arrays),
+        out_specs=(anywhere,) * len(arrays),
+        scratch_shapes=[pltpu.SemaphoreType.DMA((len(arrays),))],
+        compiler_params=pltpu.CompilerParams(vmem_limit_bytes=16 * 1024 * 1024),
+        name="finish",
+    )(*arrays)
 
 
 def routed_experts(
@@ -1124,7 +1235,7 @@
     square = paired and lax.axis_size("tp") == 8 and gate_proj.shape[0] == 1
     square = square and log_decay.shape[1] == routes.shape[0]
     if square:
-        parts, token_grad, kept = dense_experts(*args)
+        token_grad, *parts = front(*args)
     else:
         parts, token_grad, kept = routed_experts(*args)
     if square:
@@ -1138,7 +1249,8 @@
             log_decay,
             entry_state[0],
         )
-        return (*parts, *outs)
+        outs = finish(*parts, *outs)
+        return (*[part[None] for part in outs[:3]], *outs[3:])
     full_grad = lax.all_gather(token_grad, "tp", axis=1, tiled=True)
     partial = jnp.einsum(
         "td,tc->dc", full_grad, mixer_output, preferred_element_type=jnp.float32

time: 180 us -> 148 us (0.82)
  Pallas kernels: 173 us -> 142 us
    pallas_call x1, Pallas kernels: 109 us -> 96 us  [front(): pl.pallas_call(functools.partial(front_kernel, cap), out_shape=(jax.Shape...]
    pallas_call x1, Pallas kernels: 53.4 us -> 42.4 us  [tail(): pl.pallas_call(tail_kernel, out_shape=(jax.ShapeDtypeStruct((depth, colum...]
    pallas_call x1, Pallas kernels: 10.7 us -> 3.57 us  [finish(): pl.pallas_call(finish_kernel, out_shape=tuple((jax.ShapeDtypeStruct(one.s...]
    unnamed x13 -> x28, local copies, waits for them, and re-layouts: 5.88 us -> 4.87 us
where the time goes in v3:
time: 148 us
  Pallas kernels  142 us (96%)
  local copies, waits for them, and re-layouts  4.87 us (3%)
    pallas_call x1, Pallas kernels, front(): pl.pallas_call(functools.partial(front_kernel, cap), out_shape=(jax.Shape...  96 us
    pallas_call x1, Pallas kernels, tail(): pl.pallas_call(tail_kernel, out_shape=(jax.ShapeDtypeStruct((depth, colum...  42.4 us
    unnamed x28, local copies, waits for them, and re-layouts  4.87 us
    pallas_call x1, Pallas kernels, finish(): pl.pallas_call(finish_kernel, out_shape=tuple((jax.ShapeDtypeStruct(one.s...  3.57 us

profile of v3, /device:TPU:0, one launch (start us, length us, event | category | flops | bytes accessed | tf_op | source)
XLA Modules:
  0.0 147.8 jit_solution(5955730854635787202)
XLA Ops:
  0.6 0.0 copy-start.4
  0.6 0.9 copy-done.4
  1.6 0.0 copy-start.5
  1.6 0.9 copy-done.5
  2.5 0.0 copy-start.12
  2.5 0.7 copy-done.12
  3.2 0.0 copy-start.13
  3.2 0.7 copy-done.13
  3.9 0.0 copy-start
  3.9 0.0 copy-start.6
  3.9 0.0 copy-start.7
  3.9 0.0 copy-start.8
  3.9 0.0 copy-start.9
  3.9 0.0 copy-start.10
  3.9 0.0 copy-start.11
  3.9 96.0 %front.1 = (bf16[256,512]{1,0:T(8,128)(2,1)S(1)}, bf16[4096,256]{1,0:T(8,128)(2,1)}, bf16[4096,256]{1,0:T(8,128)(2,1)}, bf16[256,4096]{1,0:T(8,128)(2,1)}) custom-call(bf16[256,512]{1,0:T(8,128)(2,1)S(1)} %copy-done.4, bf16[256,512]{1,0:T(8,128)(2,1)S(1)} %copy-done.5, s32[2,256]{1,0:T(2,128)S(1)} %bitcast.7, f32[2,256]{1,0:T(2,128)S(1)} %bitcast.8, ...), custom_call_target="tpu_custom_call" | custom-call | tf_op jit(solution)/shard_map/front/pallas_call | solution.py:1079
  100.0 0.0 copy-done
  100.0 0.0 copy-done.6
  100.0 0.0 copy-done.7
  100.0 0.0 copy-done.8
  100.0 0.0 copy-done.9
  100.0 0.0 copy-done.10
  100.0 0.0 copy-done.11
  100.0 0.0 copy-start.1
  100.0 0.0 copy-start.2
  100.0 42.4 %tail.1 = (f32[1024,512]{1,0:T(8,128)S(1)}, bf16[256,256]{1,0:T(8,128)(2,1)S(1)}, bf16[256,256]{1,0:T(8,128)(2,1)S(1)}, bf16[256,512]{1,0:T(8,128)(2,1)S(1)}, f32[256,256]{1,0:T(8,128)S(1)}) custom-call(bf16[256,512]{1,0:T(8,128)(2,1)S(1)} %get-tuple-element.28.tg, bf16[4096,512]{1,0:T(8,128)(2,1)S(1)} %copy-done, bf16[256,512]{1,0:T(8,128)(2,1)S(1)} %copy-done.6, ...), custom_call_target="tpu_custom_call" | custom-call | tf_op jit(solution)/shard_map/tail/pallas_call | solution.py:608
  142.5 0.0 copy-done.1
  142.5 0.0 copy-done.2
  142.5 0.0 copy-start.3
  142.5 1.6 %copy-done.3 = bf16[256,4096]{1,0:T(8,128)(2,1)S(1)} copy-done((bf16[256,4096]{1,0:T(8,128)(2,1)S(1)}, bf16[256,4096]{1,0:T(8,128)(2,1)}, u32[]{:S(2)}) %copy-start.3) | copy-done | bytes 2097176
  144.1 3.6 %finish.1 = (bf16[4096,256]{1,0:T(8,128)(2,1)}, bf16[4096,256]{1,0:T(8,128)(2,1)}, bf16[256,4096]{1,0:T(8,128)(2,1)}, f32[1024,512]{1,0:T(8,128)}, bf16[256,256]...) custom-call(bf16[4096,256]{1,0:T(8,128)(2,1)S(1)} %copy-done.1, ...), custom_call_target="tpu_custom_call" | custom-call | tf_op jit(solution)/shard_map/finish/pallas_call | solution.py:1159
Async XLA Ops:
  0.6 1.0 copy-start.4
  1.6 0.9 copy-start.5
  2.5 0.7 copy-start.12
  3.2 0.7 copy-start.13
  3.9 96.1 %copy-start = (bf16[4096,512]{1,0:T(8,128)(2,1)S(1)}, bf16[4096,512]{1,0:T(8,128)(2,1)}, u32[]{:S(2)}) copy-start(bf16[4096,512]{1,0:T(8,128)(2,1)} %wo.1) | copy-start | bytes 12582916
  3.9 96.1 %copy-start.6 = (bf16[256,512]{1,0:T(8,128)(2,1)S(1)}, bf16[256,512]{1,0:T(8,128)(2,1)}, u32[]{:S(2)}) copy-start(bf16[256,512]{1,0:T(8,128)(2,1)} %mo.1) | copy-start | bytes 786436
  3.9 96.1 %copy-start.7 = (bf16[256,512]{1,0:T(8,128)(2,1)S(1)}, bf16[256,512]{1,0:T(8,128)(2,1)}, u32[]{:S(2)}) copy-start(bf16[256,512]{1,0:T(8,128)(2,1)} %v_ref.1) | copy-start | bytes 786436
  3.9 96.1 %copy-start.8 = (f32[256,256]{1,0:T(8,128)S(1)}, f32[256,256]{1,0:T(8,128)}, u32[]{:S(2)}) copy-start(f32[256,256]{1,0:T(8,128)} %a_ref.1) | copy-start | bytes 786436
  3.9 96.1 %copy-start.9 = (f32[1,2,128,256]{3,2,1,0:T(8,128)S(1)}, f32[1,2,128,256]{3,2,1,0:T(8,128)}, u32[]{:S(2)}) copy-start(f32[1,2,128,256]{3,2,1,0:T(8,128)} %param.27) | copy-start | bytes 786436
  3.9 96.1 %copy-start.10 = (bf16[256,256]{1,0:T(8,128)(2,1)S(1)}, bf16[256,256]{1,0:T(8,128)(2,1)}, u32[]{:S(2)}) copy-start(bf16[256,256]{1,0:T(8,128)(2,1)} %q_ref.1) | copy-start | bytes 393220
  3.9 96.1 %copy-start.11 = (bf16[256,256]{1,0:T(8,128)(2,1)S(1)}, bf16[256,256]{1,0:T(8,128)(2,1)}, u32[]{:S(2)}) copy-start(bf16[256,256]{1,0:T(8,128)(2,1)} %k_ref.1) | copy-start | bytes 393220
  100.0 42.5 %copy-start.1 = (bf16[4096,256]{1,0:T(8,128)(2,1)S(1)}, bf16[4096,256]{1,0:T(8,128)(2,1)}, u32[]{:S(2)}) copy-start(bf16[4096,256]{1,0:T(8,128)(2,1)} %get-tuple-element.25.refs_0_) | copy-start | bytes 6291460
  100.0 42.5 %copy-start.2 = (bf16[4096,256]{1,0:T(8,128)(2,1)S(1)}, bf16[4096,256]{1,0:T(8,128)(2,1)}, u32[]{:S(2)}) copy-start(bf16[4096,256]{1,0:T(8,128)(2,1)} %get-tuple-element.26.refs_1_) | copy-start | bytes 6291460
  142.5 1.6 %copy-start.3 = (bf16[256,4096]{1,0:T(8,128)(2,1)S(1)}, bf16[256,4096]{1,0:T(8,128)(2,1)}, u32[]{:S(2)}) copy-start(bf16[256,4096]{1,0:T(8,128)(2,1)} %get-tuple-element.27.refs_2_) | copy-start | bytes 6291460

commit v4 on v3

--- a/solution.py
+++ b/solution.py
@@ -1135,7 +1135,7 @@
             dma((3,)),
         ],
         compiler_params=pltpu.CompilerParams(
-            collective_id=0, has_side_effects=True, vmem_limit_bytes=52 * 1024 * 1024
+            collective_id=0, has_side_effects=True, vmem_limit_bytes=58 * 1024 * 1024
         ),
         name="front",
     )(layer_input, out_cotangent, routes.T, route_weights.T, gate_proj, up_proj, down_proj)

time: 148 us -> 147 us (level)
  local copies, waits for them, and re-layouts: 4.87 us -> 2.56 us
  Pallas kernels: 142 us -> 144 us
    unnamed x28 -> x22, local copies, waits for them, and re-layouts: 4.87 us -> 2.56 us
    pallas_call x1, Pallas kernels: 96 us -> 97.8 us  [front(): pl.pallas_call(functools.partial(front_kernel, cap), out_shape=(jax.Shape...]
where the time goes in v4:
time: 147 us
  Pallas kernels  144 us (98%)
  local copies, waits for them, and re-layouts  2.56 us (2%)
    pallas_call x1, Pallas kernels, front(): pl.pallas_call(functools.partial(front_kernel, cap), out_shape=(jax.Shape...  97.8 us
    pallas_call x1, Pallas kernels, tail(): pl.pallas_call(tail_kernel, out_shape=(jax.ShapeDtypeStruct((depth, colum...  42.4 us
    pallas_call x1, Pallas kernels, finish(): pl.pallas_call(finish_kernel, out_shape=tuple((jax.ShapeDtypeStruct(one.s...  3.57 us

profile of v4, /device:TPU:0, one launch (start us, length us, event | category | flops | bytes accessed | tf_op | source)
XLA Modules:
  0.0 147.3 jit_solution(11015799095451849578)
XLA Ops:
  0.6 0.0 copy-start
  0.6 0.0 copy-start.4
  0.7 0.0 copy-start.5
  0.7 0.0 copy-start.6
  0.7 0.0 copy-start.7
  0.7 0.0 copy-start.9
  0.7 0.0 copy-start.10
  0.7 97.8 %front.1 = (bf16[256,512]{1,0:T(8,128)(2,1)}, bf16[4096,256]{1,0:T(8,128)(2,1)}, bf16[4096,256]{1,0:T(8,128)(2,1)}, bf16[256,4096]{1,0:T(8,128)(2,1)}) custom-call(bf16[256,512]{1,0:T(8,128)(2,1)} %x_ref.1, bf16[256,512]{1,0:T(8,128)(2,1)} %g_ref.1, s32[2,256]{1,0:T(2,128)} %bitcast.7, f32[2,256]{1,0:T(2,128)} %bitcast.8, bf16[1,4096,256]{2,1,0:T(8,128)(2,1)} %wg_hbm.1, ...), custom_call_target="tpu_custom_call" | custom-call | tf_op jit(solution)/shard_map/front/pallas_call | solution.py:1079
  98.5 0.0 copy-done
  98.5 0.0 copy-done.4
  98.5 0.0 copy-done.5
  98.5 0.0 copy-done.6
  98.6 0.0 copy-done.7
  98.6 0.0 copy-done.9
  98.6 0.0 copy-done.10
  98.6 0.0 copy-start.8
  98.6 0.9 copy-done.8
  99.5 0.0 copy-start.1
  99.5 0.0 copy-start.2
  99.5 42.4 %tail.1 = (f32[1024,512]{1,0:T(8,128)S(1)}, bf16[256,256]{1,0:T(8,128)(2,1)S(1)}, bf16[256,256]{1,0:T(8,128)(2,1)S(1)}, bf16[256,512]{1,0:T(8,128)(2,1)S(1)}, f32[256,256]{1,0:T(8,128)S(1)}) custom-call(bf16[256,512]{1,0:T(8,128)(2,1)S(1)} %copy-done.8, bf16[4096,512]{1,0:T(8,128)(2,1)S(1)} %copy-done, bf16[256,512]{1,0:T(8,128)(2,1)S(1)} %copy-done.4, ...), custom_call_target="tpu_custom_call" | custom-call | tf_op jit(solution)/shard_map/tail/pallas_call | solution.py:608
  141.9 0.0 copy-done.1
  141.9 0.0 copy-done.2
  142.0 0.0 copy-start.3
  142.0 1.6 %copy-done.3 = bf16[256,4096]{1,0:T(8,128)(2,1)S(1)} copy-done((bf16[256,4096]{1,0:T(8,128)(2,1)S(1)}, bf16[256,4096]{1,0:T(8,128)(2,1)}, u32[]{:S(2)}) %copy-start.3) | copy-done | bytes 2097176
  143.5 3.6 %finish.1 = (bf16[4096,256]{1,0:T(8,128)(2,1)}, bf16[4096,256]{1,0:T(8,128)(2,1)}, bf16[256,4096]{1,0:T(8,128)(2,1)}, f32[1024,512]{1,0:T(8,128)}, bf16[256,256]...) custom-call(bf16[4096,256]{1,0:T(8,128)(2,1)S(1)} %copy-done.1, ...), custom_call_target="tpu_custom_call" | custom-call | tf_op jit(solution)/shard_map/finish/pallas_call | solution.py:1159
Async XLA Ops:
  0.6 97.9 %copy-start = (bf16[4096,512]{1,0:T(8,128)(2,1)S(1)}, bf16[4096,512]{1,0:T(8,128)(2,1)}, u32[]{:S(2)}) copy-start(bf16[4096,512]{1,0:T(8,128)(2,1)} %wo.1) | copy-start | bytes 12582916
  0.6 97.9 %copy-start.4 = (bf16[256,512]{1,0:T(8,128)(2,1)S(1)}, bf16[256,512]{1,0:T(8,128)(2,1)}, u32[]{:S(2)}) copy-start(bf16[256,512]{1,0:T(8,128)(2,1)} %mo.1) | copy-start | bytes 786436
  0.7 97.9 %copy-start.5 = (bf16[256,512]{1,0:T(8,128)(2,1)S(1)}, bf16[256,512]{1,0:T(8,128)(2,1)}, u32[]{:S(2)}) copy-start(bf16[256,512]{1,0:T(8,128)(2,1)} %v_ref.1) | copy-start | bytes 786436
  0.7 97.9 %copy-start.6 = (f32[256,256]{1,0:T(8,128)S(1)}, f32[256,256]{1,0:T(8,128)}, u32[]{:S(2)}) copy-start(f32[256,256]{1,0:T(8,128)} %a_ref.1) | copy-start | bytes 786436
  0.7 97.9 %copy-start.7 = (f32[1,2,128,256]{3,2,1,0:T(8,128)S(1)}, f32[1,2,128,256]{3,2,1,0:T(8,128)}, u32[]{:S(2)}) copy-start(f32[1,2,128,256]{3,2,1,0:T(8,128)} %param.27) | copy-start | bytes 786436
  0.7 97.9 %copy-start.9 = (bf16[256,256]{1,0:T(8,128)(2,1)S(1)}, bf16[256,256]{1,0:T(8,128)(2,1)}, u32[]{:S(2)}) copy-start(bf16[256,256]{1,0:T(8,128)(2,1)} %q_ref.1) | copy-start | bytes 393220
  0.7 97.9 %copy-start.10 = (bf16[256,256]{1,0:T(8,128)(2,1)S(1)}, bf16[256,256]{1,0:T(8,128)(2,1)}, u32[]{:S(2)}) copy-start(bf16[256,256]{1,0:T(8,128)(2,1)} %k_ref.1) | copy-start | bytes 393220
  98.6 1.0 copy-start.8
  99.5 42.4 %copy-start.1 = (bf16[4096,256]{1,0:T(8,128)(2,1)S(1)}, bf16[4096,256]{1,0:T(8,128)(2,1)}, u32[]{:S(2)}) copy-start(bf16[4096,256]{1,0:T(8,128)(2,1)} %get-tuple-element.25.refs_0_) | copy-start | bytes 6291460
  99.5 42.4 %copy-start.2 = (bf16[4096,256]{1,0:T(8,128)(2,1)S(1)}, bf16[4096,256]{1,0:T(8,128)(2,1)}, u32[]{:S(2)}) copy-start(bf16[4096,256]{1,0:T(8,128)(2,1)} %get-tuple-element.26.refs_1_) | copy-start | bytes 6291460
  142.0 1.6 %copy-start.3 = (bf16[256,4096]{1,0:T(8,128)(2,1)S(1)}, bf16[256,4096]{1,0:T(8,128)(2,1)}, u32[]{:S(2)}) copy-start(bf16[256,4096]{1,0:T(8,128)(2,1)} %get-tuple-element.27.refs_2_) | copy-start | bytes 6291460
